TPU v7x, 32 devices: a whole 2x2x4 slice. The times are simulated.
32 devices in a mesh: sp: 4 (over y, x), tp: 8 (over z, core).
Axes of the slice: x: 2, y: 2, z: 4, core: 2. Of those that a mesh axis runs over, the one named last changes fastest.
Arguments:
- moe_input: bfloat16 [512, 2048], P('sp'), may hold values from -6 to 6
- cotangent: bfloat16 [512, 2048], P('sp'), may hold values from -6 to 6
- route_expert: int32 [512, 2], P('sp'), may hold values from 0 to 3, all different within a row; in each aligned block of 128 rows (0 to 127, 128 to 255, ...) at most 128 rows name the same one
- route_weight: float32 [512, 2], P('sp'), may hold values from 0.2 to 1
- w_gate: bfloat16 [4, 2048, 6144], P('sp', None, 'tp'), may hold values from -0.125 to 0.125
- w_up: bfloat16 [4, 2048, 6144], P('sp', None, 'tp'), may hold values from -0.125 to 0.125
- w_down: bfloat16 [4, 6144, 2048], P('sp', 'tp'), may hold values from -0.078125 to 0.078125
- out_proj: bfloat16 [2048, 2048], P('tp'), may hold values from -0.125 to 0.125
- saved_out: bfloat16 [512, 2048], P('sp', 'tp'), may hold values from -6 to 6
- queries: bfloat16 [512, 1024], P('sp', 'tp'), may hold values from -6 to 6
- keys: bfloat16 [512, 1024], P('sp', 'tp'), may hold values from -6 to 6
- values: bfloat16 [512, 2048], P('sp', 'tp'), may hold values from -6 to 6
- log_decay: float32 [512, 1024], P('sp', 'tp'), may hold values from -1 to 0
- span_state: float32 [8, 1024, 128], P('sp', 'tp'), may hold values from -6 to 6
Outputs:
- grad_w_gate: bfloat16 [4, 2048, 6144], P('sp', None, 'tp')
- grad_w_up: bfloat16 [4, 2048, 6144], P('sp', None, 'tp')
- grad_w_down: bfloat16 [4, 6144, 2048], P('sp', 'tp')
- grad_proj: float32 [2048, 2048], P('sp', 'tp')
- grad_queries: bfloat16 [512, 1024], P('sp', 'tp')
- grad_keys: bfloat16 [512, 1024], P('sp', 'tp')
- grad_values: bfloat16 [512, 2048], P('sp', 'tp')
- grad_decay: float32 [512, 1024], P('sp', 'tp')
Inputs may be any that keep to these rules, and one draw needn't show every extreme that they name: `route_expert`: each row names two different experts. Within the 128 rows of one index of sp no expert is named by more than 128 rows, a bound that some block reaches.
All inputs are finite; a program needn't handle non-finite values.
Results may differ from a plain program's by a relative error of at most 0.019.
Values may be sent and summed in bfloat16 or wider, within the bound.
A program may use at most 128 MiB of HBM per device.

v0:
```python
import functools

import jax
import jax.numpy as jnp
from jax import lax
from jax.experimental import pallas as pl
from jax.experimental.pallas import tpu as pltpu
from jax.sharding import PartitionSpec as P

DK = 64
SPAN = 64

HIGH = lax.Precision.HIGHEST
F32 = jnp.float32
BF16 = jnp.bfloat16


def dot(a, b, dims, precision=HIGH):
    return lax.dot_general(
        a, b, ((dims[0], dims[1]), ((), ())), precision=precision, preferred_element_type=F32
    )


NN = ((1,), (0,))
NT = ((1,), (1,))
TN = ((0,), (0,))


def triangle(size, upper):
    row = lax.broadcasted_iota(jnp.int32, (size, size), 0)
    col = lax.broadcasted_iota(jnp.int32, (size, size), 1)
    return ((row <= col) if upper else (row >= col)).astype(F32)


def there(sp=None, tp=None):
    where = {}
    if sp is not None:
        where["sp"] = sp
    if tp is not None:
        where["tp"] = tp
    return where


def greet(partners):
    barrier = pltpu.get_barrier_semaphore()
    for partner in partners:
        pl.semaphore_signal(
            barrier, inc=1, device_id=partner, device_id_type=pl.DeviceIdType.MESH
        )
    pl.semaphore_wait(barrier, len(partners))


def send(src, dst, sems, slot, partner):
    copy = pltpu.make_async_remote_copy(
        src_ref=src,
        dst_ref=dst,
        send_sem=sems[0].at[slot],
        recv_sem=sems[1].at[slot],
        device_id=partner,
        device_id_type=pl.DeviceIdType.MESH,
    )
    copy.start()
    return copy


def gather_kernel(n, own_a, own_b, weights, decays, all_a, all_b, all_w, all_d, *sems):
    me, lane = lax.axis_index("sp"), lax.axis_index("tp")
    core = lax.rem(lane, 2)
    twin = there(tp=lane + 1 - 2 * core)
    rows = own_a.shape[0]
    half = rows // 2
    peers = [there(sp=lax.rem(me + d, n)) for d in range(1, n)]
    greet(peers + [twin])
    far, near = sems[:2], sems[2:4]
    copies = []
    for t, (own, full) in enumerate([(weights, all_w), (decays, all_d)]):
        for d, peer in enumerate(peers):
            copies.append(send(own, full.at[me], far, t * (n - 1) + d, peer))
    bulk = []
    pieces = pl.ds(pl.multiple_of(core * half, half), half)
    for t, (own, full) in enumerate([(own_a, all_a), (own_b, all_b)]):
        for d, peer in enumerate(peers):
            at = pl.ds(pl.multiple_of(me * rows + core * half, half), half)
            bulk.append(send(own.at[pieces], full.at[at], far, (t + 2) * (n - 1) + d, peer))
    here = pl.ds(pl.multiple_of(me * rows, rows), rows)
    all_a[here, :] = own_a[...]
    all_b[here, :] = own_b[...]
    all_w[me] = weights[...]
    all_d[me] = decays[...]
    for t, full in enumerate([all_a, all_b]):
        for d in range(n - 1):
            slot = t * (n - 1) + d
            bulk[slot].wait_recv()
            source = lax.rem(me + n - 1 - d, n)
            at = pl.ds(pl.multiple_of(source * rows + core * half, half), half)
            copies.append(send(full.at[at], full.at[at], near, slot, twin))
    for copy in bulk:
        copy.wait_send()
    for copy in copies:
        copy.wait()


def sum_kernel(n, slots, cot, out, got_a, sum_a, got_b, sum_b, got_c, *sems):
    me, lane = lax.axis_index("sp"), lax.axis_index("tp")
    core = lax.rem(lane, 2)
    z = lax.div(lane, 2)
    half = got_a.shape[1]
    depth = got_c.shape[0] + 1
    piece = half // depth
    rows = 2 * half
    twin = there(tp=lane + 1 - 2 * core)
    peers = [there(sp=lax.rem(me + d, n)) for d in range(1, n)]
    along = [lax.rem(z + d, depth) for d in range(1, depth)]
    lanes = [there(tp=2 * other + core) for other in along]
    greet(peers + lanes + [twin])
    a, b, c, d_, e = (sems[2 * i : 2 * i + 2] for i in range(5))

    def rows_at(start, size):
        return pl.ds(pl.multiple_of(start, size), size)

    first = [
        send(slots.at[rows_at(k * rows + (1 - core) * half, half)], got_a.at[k], a, k, twin)
        for k in range(n)
    ]
    for k in range(n):
        first[k].wait_recv()
        mine = slots[rows_at(k * rows + core * half, half), :].astype(F32)
        sum_a[k] = (mine + got_a[k].astype(F32)).astype(BF16)
    second = [
        send(sum_a.at[lax.rem(me + d, n)], got_b.at[d - 1], b, d - 1, peers[d - 1])
        for d in range(1, n)
    ]
    total = sum_a[me].astype(F32)
    for d in range(n - 1):
        second[d].wait_recv()
        total = total + got_b[d].astype(F32)
    sum_b[...] = total.astype(BF16)
    third = [
        send(sum_b.at[rows_at(along[d] * piece, piece)], got_c.at[d], c, d, lanes[d])
        for d in range(depth - 1)
    ]
    mine = rows_at(core * half + z * piece, piece)
    total = cot[mine, :].astype(F32) + sum_b[rows_at(z * piece, piece), :].astype(F32)
    for d in range(depth - 1):
        third[d].wait_recv()
        total = total + got_c[d].astype(F32)
    out[mine, :] = total.astype(BF16)
    fourth = [send(out.at[mine], out.at[mine], d_, d, lanes[d]) for d in range(depth - 1)]
    for copy in fourth:
        copy.wait_recv()
    whole = rows_at(core * half, half)
    fifth = send(out.at[whole], out.at[whole], e, 0, twin)
    fifth.wait()
    for copy in first + second + third + fourth:
        copy.wait_send()


def mix_kernel(n, grad_in, out_proj, queries, log_decay, mix_out, starts, *sems):
    me = lax.axis_index("sp")
    peers = [there(sp=lax.rem(me + d, n)) for d in range(1, n)]
    greet(peers)
    mix = dot(grad_in[...], out_proj[...], NT, None)
    mix_out[...] = mix
    rows, channels = queries.shape
    heads = channels // DK
    wide = mix.shape[1] // heads
    lower = triangle(SPAN, False)
    ones = jnp.ones((SPAN, wide), F32)
    for h in range(heads):
        keyed = slice(h * DK, (h + 1) * DK)
        carry = None
        for n_ in reversed(range(rows // SPAN)):
            at = slice(n_ * SPAN, (n_ + 1) * SPAN)
            decay = log_decay[at, keyed]
            qd = queries[at, keyed].astype(F32) * jnp.exp(dot(lower, decay, NN))
            local = DK**-0.5 * dot(qd, mix[at, h * wide : (h + 1) * wide], TN)
            if carry is not None:
                local = local + jnp.exp(dot(decay, ones, TN)) * carry
            carry = local
        starts[me, keyed, :] = carry
    copies = [send(starts.at[me], starts.at[me], sems, d, peers[d]) for d in range(n - 1)]
    for copy in copies:
        copy.wait()


def weight_kernel(inputs, routed, hidden, d_gate, d_upper, gate_o, up_o, down_o):
    gate_o[0] = dot(inputs[...], d_gate[...], TN, None).astype(BF16)
    up_o[0] = dot(inputs[...], d_upper[...], TN, None).astype(BF16)
    down_o[0] = dot(hidden[...], routed[...], TN, None).astype(BF16)


def weight_grads(inputs, routed, hidden, d_gate, d_upper):
    slots, width = inputs.shape
    units = hidden.shape[1]
    tile = width // 8
    moving = pl.BlockSpec((slots, tile), lambda i: (0, i))
    still = pl.BlockSpec((slots, units), lambda i: (0, 0))
    return pl.pallas_call(
        weight_kernel,
        grid=(width // tile,),
        out_shape=[
            jax.ShapeDtypeStruct((1, width, units), BF16),
            jax.ShapeDtypeStruct((1, width, units), BF16),
            jax.ShapeDtypeStruct((1, units, width), BF16),
        ],
        in_specs=[moving, moving, still, still, still],
        out_specs=[
            pl.BlockSpec((1, tile, units), lambda i: (0, i, 0)),
            pl.BlockSpec((1, tile, units), lambda i: (0, i, 0)),
            pl.BlockSpec((1, units, tile), lambda i: (0, 0, i)),
        ],
        cost_estimate=pl.CostEstimate(
            flops=6 * slots * width * units,
            bytes_accessed=6 * width * units,
            transcendentals=0,
        ),
    )(inputs, routed, hidden, d_gate, d_upper)


def finish_kernel(queries, keys, values, log_decay, mix, state, after, dq_o, dk_o, dv_o, dl_o):
    rows, channels = queries.shape
    heads = channels // DK
    wide = values.shape[1] // heads
    lower = triangle(SPAN, False)
    upper = triangle(SPAN, True)
    ones = jnp.ones((SPAN, wide), F32)
    scale = DK**-0.5
    for h in range(heads):
        keyed = slice(h * DK, (h + 1) * DK)
        valued = slice(h * wide, (h + 1) * wide)
        g_end = after[keyed, :]
        for n in reversed(range(rows // SPAN)):
            at = slice(n * SPAN, (n + 1) * SPAN)
            q = queries[at, keyed].astype(F32)
            k = keys[at, keyed].astype(F32)
            v = values[at, valued].astype(F32)
            g = mix[at, valued]
            s0 = state[n, keyed, :]
            decay = log_decay[at, keyed]
            c = dot(lower, decay, NN)
            last = c[SPAN - 1 : SPAN, :]
            grow, shrink, to_end = jnp.exp(c), jnp.exp(-c), jnp.exp(last - c)
            qd, kd, ke = q * grow, k * shrink, k * to_end
            scores = dot(qd, kd, NT) * lower
            gv = dot(g, v, NT) * lower
            dq = scale * grow * (dot(gv, kd, NN) + dot(g, s0, NT))
            dk = scale * shrink * dot(gv, qd, TN) + to_end * dot(v, g_end, NT)
            dv = scale * dot(scores, g, TN) + dot(ke, g_end, NN)
            e_last = jnp.exp(dot(decay, ones, TN))
            s1 = e_last * s0 + dot(ke, v, TN)
            dq_o[at, keyed] = dq.astype(BF16)
            dk_o[at, keyed] = dk.astype(BF16)
            dv_o[at, valued] = dv.astype(BF16)
            dl_o[at, keyed] = dot(upper, q * dq - k * dk, NN) + dot(ones, s1 * g_end, NT)
            if n:
                g_end = DK**-0.5 * dot(qd, g, TN) + e_last * g_end


def call(kernel, outs, *args, scratch=(), sems=(), ident=None):
    semaphores = [pltpu.SemaphoreType.DMA((count,)) for count in sems for _ in range(2)]
    return pl.pallas_call(
        kernel,
        out_shape=[jax.ShapeDtypeStruct(s, d) for s, d in outs],
        in_specs=[pl.BlockSpec(memory_space=pltpu.VMEM)] * len(args),
        out_specs=[pl.BlockSpec(memory_space=pltpu.VMEM)] * len(outs),
        scratch_shapes=[pltpu.VMEM(s, BF16) for s in scratch] + semaphores,
        cost_estimate=pl.CostEstimate(flops=2 * 10**8, bytes_accessed=10**6, transcendentals=0),
        compiler_params=pltpu.CompilerParams(
            collective_id=ident, has_side_effects=ident is not None
        ),
    )(*args)


def on_device(
    moe_input,
    cotangent,
    route_expert,
    route_weight,
    w_gate,
    w_up,
    w_down,
    out_proj,
    saved_out,
    queries,
    keys,
    values,
    log_decay,
    span_state,
):
    tok_rows, width = moe_input.shape
    groups = lax.axis_size("sp")
    lanes = lax.axis_size("tp")
    me = lax.axis_index("sp")
    named = route_expert[:, :, None] == jnp.arange(groups, dtype=jnp.int32)
    weights = jnp.sum(jnp.where(named, route_weight[:, :, None], 0.0), axis=1).T
    decay_sum = jnp.sum(log_decay, axis=0, keepdims=True)
    inputs, cots, weights_all, decays = call(
        functools.partial(gather_kernel, groups),
        [
            ((groups * tok_rows, width), BF16),
            ((groups * tok_rows, width), BF16),
            ((groups, groups, tok_rows), F32),
            ((groups, 1, log_decay.shape[1]), F32),
        ],
        moe_input,
        cotangent,
        weights,
        decay_sum,
        sems=(4 * (groups - 1), 2 * (groups - 1)),
        ident=1,
    )
    mine = lax.dynamic_index_in_dim(weights_all, me, 1, keepdims=False).reshape(-1, 1)
    decays = decays[:, 0]

    gate_weight, up_weight, down_weight = w_gate[0], w_up[0], w_down[0]
    gate = jnp.dot(inputs, gate_weight, preferred_element_type=F32)
    upper = jnp.dot(inputs, up_weight, preferred_element_type=F32)
    routed = (mine * cots.astype(F32)).astype(BF16)
    sigmoid_gate = jax.nn.sigmoid(gate)
    active = gate * sigmoid_gate
    hidden = (active * upper).astype(BF16)
    d_hidden = dot(routed, down_weight, NT, None)
    d_upper = (d_hidden * active).astype(BF16)
    d_gate = (d_hidden * upper * sigmoid_gate * (1.0 + gate * (1.0 - sigmoid_gate))).astype(BF16)
    slots = (dot(d_gate, gate_weight, NT, None) + dot(d_upper, up_weight, NT, None)).astype(BF16)
    half, depth = tok_rows // 2, lanes // 2
    (grad_in,) = call(
        functools.partial(sum_kernel, groups),
        [((tok_rows, width), BF16)],
        slots,
        cotangent,
        scratch=[
            (groups, half, width),
            (groups, half, width),
            (groups - 1, half, width),
            (half, width),
            (depth - 1, half // depth, width),
        ],
        sems=(groups, groups - 1, depth - 1, depth - 1, 1),
        ident=2,
    )
    proj = dot(grad_in, saved_out, TN, None).astype(BF16)
    hidden, proj = lax.optimization_barrier((hidden, proj))
    grad_gate, grad_up, grad_down = weight_grads(inputs, routed, hidden, d_gate, d_upper)
    queries_late, grad_up = lax.optimization_barrier((queries, grad_up))

    channels, wide = queries.shape[1], span_state.shape[2]
    mix, starts = call(
        functools.partial(mix_kernel, groups),
        [((tok_rows, values.shape[1]), F32), ((groups, channels, wide), F32)],
        grad_in,
        out_proj,
        queries_late,
        log_decay,
        sems=(groups - 1,),
        ident=3,
    )
    grad_proj = lax.psum_scatter(
        proj, "sp", scatter_dimension=0, tiled=True
    ).astype(F32)
    at = jnp.arange(groups, dtype=jnp.int32)
    between = ((at[None, :] > me) & (at[None, :] < at[:, None])).astype(F32)
    factor = jnp.exp(jnp.sum(between[:, :, None] * decays[None], axis=1))
    factor = jnp.where((at > me)[:, None], factor, 0.0)
    after = jnp.sum(factor[:, :, None] * starts, axis=0)
    grad_queries, grad_keys, grad_values, grad_decay = call(
        finish_kernel,
        [
            (queries.shape, BF16),
            (keys.shape, BF16),
            (values.shape, BF16),
            (log_decay.shape, F32),
        ],
        queries,
        keys,
        values,
        log_decay,
        mix,
        span_state,
        after,
    )
    return (
        grad_gate,
        grad_up,
        grad_down,
        grad_proj,
        grad_queries,
        grad_keys,
        grad_values,
        grad_decay,
    )


def solution(mesh):
    placed = (
        P("sp", None),
        P("sp", None),
        P("sp", None),
        P("sp", None),
        P("sp", None, "tp"),
        P("sp", None, "tp"),
        P("sp", "tp", None),
        P("tp", None),
        P("sp", "tp"),
        P("sp", "tp"),
        P("sp", "tp"),
        P("sp", "tp"),
        P("sp", "tp"),
        P("sp", "tp", None),
    )
    return jax.shard_map(
        on_device,
        mesh=mesh,
        in_specs=placed,
        out_specs=(
            P("sp", None, "tp"),
            P("sp", None, "tp"),
            P("sp", "tp", None),
            P("sp", "tp"),
            P("sp", "tp"),
            P("sp", "tp"),
            P("sp", "tp"),
            P("sp", "tp"),
        ),
        check_vma=False,
    )
```

profile of v0, /device:TPU:0, one launch (start us, length us, event | category | flops | bytes accessed | tf_op | source)
XLA Modules:
  0.0 134.9 jit_solution(7271559853256237410)
XLA Ops:
  7.2 0.0 copy-start
  7.2 0.0 reduce-scatter.2.cloned.1.call-start
  7.2 1.5 %reduce_sum.37 = f32[128]{0:T(128)} reduce(f32[128,128]{1,0:T(8,128)} %log_decay.3, f32[]{:T(128)} %constant.5.clone.1), dimensions={0}, to_apply=%region_1.2 | reduce | flops 16256 | bytes 66052 | tf_op jit(solution)/shard_map/reduce_sum | solution.py:296
  8.8 1.3 select_reduce_fusion
  10.0 32.5 %shard_map.197 = (bf16[512,2048]{1,0:T(8,128)(2,1)}, bf16[512,2048]{1,0:T(8,128)(2,1)}, f32[4,4,128]{2,1,0:T(4,128)}, f32[4,1,128]{2,1,0:T(1,128)}) custom-call(bf16[128,2048]{1,0:T(8,128)(2,1)} %own_a.1, bf16[128,2048]{1,0:T(8,128)(2,1)} %cot.1, f32[4,128]{1,0:T(4,128)} %bitcast.28, f32[1,128]{1,0:T(1,128)} %bitcast.30), custom_call_target="tpu_custom_call" | custom-call | flops 200000000 | bytes 1000000 | tf_op jit(solution)/shard_map/pallas_call | solution.py:261
  42.6 0.7 constant_dynamic-slice_fusion
  43.3 2.1 %multiply_convert_fusion.routed = bf16[512,2048]{1,0:T(8,128)(2,1)S(1)} fusion(bf16[512,2048]{1,0:T(8,128)(2,1)} %get-tuple-element.27, f32[512]{0:T(512)S(1)} %bitcast.29), kind=kLoop, calls=%fused_computation.1 | loop fusion | flops 3145728 | bytes 4196352 | tf_op jit(solution)/shard_map/convert_element_type | solution.py:318
  45.4 0.4 copy-done.4
  45.8 1.8 %fusion = f32[512,768]{1,0:T(8,128)S(1)} fusion(bf16[512,2048]{1,0:T(8,128)(2,1)S(1)} %multiply_convert_fusion.routed, bf16[1,768,2048]{2,1,0:T(8,128)(2,1)S(1)} %copy-done.4), kind=kOutput, calls=%fused_computation.2 | convolution fusion | flops 1610612736 | bytes 6815744 | tf_op jit(solution)/shard_map/dot_general | solution.py:19
  47.6 0.0 copy-done.1
  47.6 0.8 copy-done.5
  48.4 0.6 copy-done.6
  49.1 1.8 %fusion.4 = f32[512,768]{1,0:T(8,128)S(1)} fusion(bf16[512,2048]{1,0:T(8,128)(2,1)S(1)} %copy-done.6, bf16[1,2048,768]{2,1,0:T(8,128)(2,1)S(1)} %copy-done.5), kind=kOutput, calls=%fused_computation.6 | convolution fusion | flops 1610612736 | bytes 6815744 | tf_op jit(solution)/shard_map/dot_general | solution.py:317
  50.9 0.0 copy-done
  50.9 3.3 %multiply_convert_fusion.2 = (bf16[512,768]{1,0:T(8,128)(2,1)S(1)}, bf16[512,768]{1,0:T(8,128)(2,1)S(1)}, bf16[512,768]{1,0:T(8,128)(2,1)}) fusion(f32[512,768]{1,0:T(8,128)S(1)} %fusion, f32[512,768]{1,0:T(8,128)S(1)} %fusion.4, bf16[512,2048]{1,0:T(8,128)(2,1)S(1)} %copy-done.6, bf16[1,2048,768]{2,1,0:T(8,128)(2,1)S(1)} %copy-done), kind=kOutput, calls=%fused_computation.14 | convolution fusion | flops 1616510976 | bytes 10747904 | tf_op jit(solution)/shard_map/dot_general | solution.py:316
  54.2 1.8 %fusion.2 = f32[512,2048]{1,0:T(8,128)S(1)} fusion(bf16[512,768]{1,0:T(8,128)(2,1)S(1)} %get-tuple-element.43.d_upper, bf16[1,2048,768]{2,1,0:T(8,128)(2,1)S(1)} %copy-done.5), kind=kOutput, calls=%fused_computation.4 | convolution fusion | flops 1610612736 | bytes 8126464 | tf_op jit(solution)/shard_map/dot_general | solution.py:19
  56.0 0.0 copy-done.8
  56.1 0.0 copy-done.7
  56.1 3.2 %add_convert_fusion.slots = bf16[512,2048]{1,0:T(8,128)(2,1)} fusion(f32[512,2048]{1,0:T(8,128)S(1)} %fusion.2, bf16[512,768]{1,0:T(8,128)(2,1)S(1)} %get-tuple-element.42.d_gate, bf16[1,2048,768]{2,1,0:T(8,128)(2,1)S(1)} %copy-done), kind=kOutput, calls=%fused_computation | convolution fusion | flops 1612709888 | bytes 10223616 | tf_op jit(solution)/shard_map/dot_general | solution.py:19
  59.2 35.6 %shard_map.198.grad_in = bf16[128,2048]{1,0:T(8,128)(2,1)} custom-call(bf16[512,2048]{1,0:T(8,128)(2,1)} %add_convert_fusion.slots, bf16[128,2048]{1,0:T(8,128)(2,1)} %cot.1), custom_call_target="tpu_custom_call" | custom-call | flops 200000000 | bytes 1000000 | tf_op jit(solution)/shard_map/pallas_call | solution.py:261
  94.8 0.0 copy-done.2
  94.9 2.5 %convolution_convert_fusion = bf16[2048,256]{1,0:T(8,128)(2,1)} fusion(bf16[128,2048]{1,0:T(8,128)(2,1)} %shard_map.198.grad_in, bf16[128,256]{1,0:T(8,128)(2,1)S(1)} %copy-done.2), kind=kOutput, calls=%fused_computation.12 | convolution fusion | flops 134742016 | bytes 1638400 | tf_op jit(solution)/shard_map/dot_general | solution.py:19
  97.3 0.0 reduce-scatter.2.cloned.1.call-update
  97.4 0.0 copy-start.3
  97.4 10.5 %shard_map.199 = (bf16[1,2048,768]{2,1,0:T(8,128)(2,1)}, bf16[1,2048,768]{2,1,0:T(8,128)(2,1)}, bf16[1,768,2048]{2,1,0:T(8,128)(2,1)}) custom-call(bf16[512,2048]{1,0:T(8,128)(2,1)} %get-tuple-element.25.inputs, bf16[512,2048]{1,0:T(8,128)(2,1)} %copy-done.1, bf16[512,768]{1,0:T(8,128)(2,1)} %get-tuple-element.28.hidden, bf16[512,768]{1,0:T(8,128)(2,1)} %copy-done.7, ...), custom_call_target="tpu_custom_call" | custom-call | flops 4831838208 | bytes 9437184 | tf_op jit(solution)/shard_map/pallas_call | solution.py:198
  107.9 11.0 %shard_map.200 = (f32[128,256]{1,0:T(8,128)}, f32[4,128,128]{2,1,0:T(8,128)}) custom-call(bf16[128,2048]{1,0:T(8,128)(2,1)} %shard_map.198.grad_in, bf16[256,2048]{1,0:T(8,128)(2,1)} %out_proj.1, bf16[128,128]{1,0:T(8,128)(2,1)} %queries.2, f32[128,128]{1,0:T(8,128)} %log_decay.3), custom_call_target="tpu_custom_call" | custom-call | flops 200000000 | bytes 1000000 | tf_op jit(solution)/shard_map/pallas_call | solution.py:261
  119.0 0.0 copy-done.3
  119.0 0.1 multiply_reduce_fusion.1
  119.1 0.1 exponential_select_fusion
  119.1 1.7 %multiply_reduce_fusion.after = f32[128,128]{1,0:T(8,128)} fusion(f32[4,128,128]{2,1,0:T(8,128)} %get-tuple-element.37, f32[4,128]{1,0:T(4,128)S(1)} %exponential_select_fusion), kind=kLoop, calls=%fused_computation.18 | loop fusion | flops 114688 | bytes 329728 | tf_op jit(solution)/shard_map/reduce_sum | solution.py:365
  120.9 5.4 %shard_map.201 = (bf16[128,128]{1,0:T(8,128)(2,1)}, bf16[128,128]{1,0:T(8,128)(2,1)}, bf16[128,256]{1,0:T(8,128)(2,1)}, f32[128,128]{1,0:T(8,128)}) custom-call(bf16[128,128]{1,0:T(8,128)(2,1)} %queries.2, bf16[128,128]{1,0:T(8,128)(2,1)} %keys.1, bf16[128,256]{1,0:T(8,128)(2,1)} %values.1, f32[128,128]{1,0:T(8,128)} %log_decay.3, ...), custom_call_target="tpu_custom_call" | custom-call | flops 200000000 | bytes 1000000 | tf_op jit(solution)/shard_map/pallas_call | solution.py:261
  126.3 1.8 %convert_element_type.38 = f32[512,256]{1,0:T(8,128)} convert(bf16[512,256]{1,0:T(8,128)(2,1)} %reduce-scatter.2.cloned.1.call-done) | non-fusion elementwise | flops 131072 | bytes 786432 | tf_op jit(solution)/shard_map/convert_element_type | solution.py:360
  (10 shorter events, 0.0 us)
Async XLA Ops:
  7.2 43.7 %copy-start = (bf16[1,2048,768]{2,1,0:T(8,128)(2,1)S(1)}, bf16[1,2048,768]{2,1,0:T(8,128)(2,1)}, u32[]{:S(2)}) copy-start(bf16[1,2048,768]{2,1,0:T(8,128)(2,1)} %param.18) | copy-start | bytes 9437188
  7.2 119.1 %reduce-scatter.2.cloned.1.call-start = ((), (), s32[]{:S(2)}) async-start(), calls=%async_computation.1 | async-start | bytes 1310720 | tf_op jit(solution)/shard_map/reduce_scatter | solution.py:358
  43.3 2.5 %copy-start.4 = (bf16[1,768,2048]{2,1,0:T(8,128)(2,1)S(1)}, bf16[1,768,2048]{2,1,0:T(8,128)(2,1)}, u32[]{:S(2)}) copy-start(bf16[1,768,2048]{2,1,0:T(8,128)(2,1)} %param.20) | copy-start | bytes 9437188
  45.8 1.8 %copy-start.1 = (bf16[512,2048]{1,0:T(8,128)(2,1)}, bf16[512,2048]{1,0:T(8,128)(2,1)S(1)}, u32[]{:S(2)}) copy-start(bf16[512,2048]{1,0:T(8,128)(2,1)S(1)} %multiply_convert_fusion.routed) | copy-start | bytes 6291460
  45.8 2.6 %copy-start.5 = (bf16[1,2048,768]{2,1,0:T(8,128)(2,1)S(1)}, bf16[1,2048,768]{2,1,0:T(8,128)(2,1)}, u32[]{:S(2)}) copy-start(bf16[1,2048,768]{2,1,0:T(8,128)(2,1)} %param.19) | copy-start | bytes 9437188
  45.8 3.3 %copy-start.6 = (bf16[512,2048]{1,0:T(8,128)(2,1)S(1)}, bf16[512,2048]{1,0:T(8,128)(2,1)}, u32[]{:S(2)}) copy-start(bf16[512,2048]{1,0:T(8,128)(2,1)} %get-tuple-element.25.inputs) | copy-start | bytes 6291460
  54.2 1.8 %copy-start.8 = (bf16[512,768]{1,0:T(8,128)(2,1)}, bf16[512,768]{1,0:T(8,128)(2,1)S(1)}, u32[]{:S(2)}) copy-start(bf16[512,768]{1,0:T(8,128)(2,1)S(1)} %get-tuple-element.43.d_upper) | copy-start | bytes 2359300
  54.2 1.8 %copy-start.7 = (bf16[512,768]{1,0:T(8,128)(2,1)}, bf16[512,768]{1,0:T(8,128)(2,1)S(1)}, u32[]{:S(2)}) copy-start(bf16[512,768]{1,0:T(8,128)(2,1)S(1)} %get-tuple-element.42.d_gate) | copy-start | bytes 2359300
  59.2 35.6 %copy-start.2 = (bf16[128,256]{1,0:T(8,128)(2,1)S(1)}, bf16[128,256]{1,0:T(8,128)(2,1)}, u32[]{:S(2)}) copy-start(bf16[128,256]{1,0:T(8,128)(2,1)} %param.22) | copy-start | bytes 196612
  97.4 21.6 %copy-start.3 = (f32[4,1,128]{2,1,0:T(1,128)S(1)}, f32[4,1,128]{2,1,0:T(1,128)}, u32[]{:S(2)}) copy-start(f32[4,1,128]{2,1,0:T(1,128)} %get-tuple-element.36) | copy-start | bytes 6148
Sparse Core Ops, SparseCore 0:
  97.5 28.6 reduce-scatter.1
where the time goes:
time: 135 us
  Pallas kernels  95.1 us (70%)
  matrix products  14.4 us (11%)
  between operations  14.2 us (11%)
  other arithmetic  8.63 us (6%)
  local copies, waits for them, and re-layouts  2.55 us (2%)
    pallas_call x4, Pallas kernels, call(): pl.pallas_call(kernel, out_shape=[jax.ShapeDtypeStruct(s, d) for s, d in...  84.6 us
    pallas_call x1, Pallas kernels, weight_grads(): pl.pallas_call(weight_kernel, grid=(width // tile,), out_shape=[jax.Shape...  10.5 us
    dot_general x4, matrix products, dot(): lax.dot_general(a, b, ((dims[0], dims[1]), ((), ())), precision=precision...  9.3 us
    dot_general x1, matrix products, on_device(): gate = jnp.dot(inputs, gate_weight, preferred_element_type=F32)  3.31 us
  transfers between devices with their start and end apart: 1, of which 0 were waited for; matrix products, arithmetic and copies ran while one was open for 1% of the time, Pallas kernels for 20%

commit v1 on v0

v1 whole, which is shorter than its diff:
```python
import functools
import math

import jax
import jax.numpy as jnp
from jax import lax
from jax.experimental import pallas as pl
from jax.experimental.pallas import tpu as pltpu
from jax.sharding import PartitionSpec as P

DK = 64
SPAN = 64

HIGH = lax.Precision.HIGHEST
F32 = jnp.float32
BF16 = jnp.bfloat16


def dot(a, b, dims, precision=HIGH):
    return lax.dot_general(
        a, b, ((dims[0], dims[1]), ((), ())), precision=precision, preferred_element_type=F32
    )


NN = ((1,), (0,))
NT = ((1,), (1,))
TN = ((0,), (0,))


def triangle(size, upper):
    row = lax.broadcasted_iota(jnp.int32, (size, size), 0)
    col = lax.broadcasted_iota(jnp.int32, (size, size), 1)
    return ((row <= col) if upper else (row >= col)).astype(F32)


def there(sp=None, tp=None):
    where = {}
    if sp is not None:
        where["sp"] = sp
    if tp is not None:
        where["tp"] = tp
    return where


def greet(partners):
    barrier = pltpu.get_barrier_semaphore()
    for partner in partners:
        pl.semaphore_signal(
            barrier, inc=1, device_id=partner, device_id_type=pl.DeviceIdType.MESH
        )
    pl.semaphore_wait(barrier, len(partners))


def send(src, dst, sems, slot, partner):
    copy = pltpu.make_async_remote_copy(
        src_ref=src,
        dst_ref=dst,
        send_sem=sems[0].at[slot],
        recv_sem=sems[1].at[slot],
        device_id=partner,
        device_id_type=pl.DeviceIdType.MESH,
    )
    copy.start()
    return copy


def expert_kernel(
    n, depth, moe, cot, saved, experts, shares, decay, gate_h, up_h, down_h,
    grad_in, all_s, packet, gate_o, up_o, down_o,
    all_a, all_b, routed, hidden, d_gate, d_upper, gate_w, up_w, down_w,
    slots, got_t, got_p, sum_z, got_z, local, *sems,
):
    me, lane = lax.axis_index("sp"), lax.axis_index("tp")
    core, z = lax.rem(lane, 2), lax.div(lane, 2)
    side = math.isqrt(n)
    y, x = lax.div(me, side), lax.rem(me, side)
    rows, width = moe.shape
    units = hidden.shape[1]
    channels = decay.shape[1]
    split = rows // 2
    wide = width // 2
    part = wide // 2
    piece = rows // depth
    far, near, small, twin_s, plane_s, z_s, back_s, twin_b = (
        sems[2 * i : 2 * i + 2] for i in range(8)
    )

    def ds(start, size):
        return pl.ds(pl.multiple_of(start, size), size)

    def place(dy, dx):
        return lax.rem(y + dy + side, side) * side + lax.rem(x + dx + side, side)

    def half(block):
        return ds(block * rows + core * split, split)

    def whole(block):
        return ds(block * rows, rows)

    started = []

    def go(*args):
        copy = send(*args)
        started.append(copy)
        return copy

    twin = there(tp=lane + 1 - 2 * core)
    peers = [there(sp=lax.rem(me + d, n)) for d in range(1, n)]
    along = [lax.rem(z + d, depth) for d in range(1, depth)]
    lanes = [there(tp=2 * far_z + core) for far_z in along]
    loads = [
        pltpu.make_async_copy(src, dst, local.at[i])
        for i, (src, dst) in enumerate([
            (moe, all_a.at[whole(me)]),
            (cot, all_b.at[whole(me)]),
            (gate_h.at[0], gate_w),
            (up_h.at[0], up_w),
            (down_h.at[0], down_w),
            (saved, all_s.at[whole(me)]),
        ])
    ]
    for load in loads:
        load.start()
    index = lax.broadcasted_iota(jnp.int32, (n, rows), 0)
    packet[me, 0:n, :] = jnp.where(index == experts[0:1, :], shares[0:1, :], 0.0) + jnp.where(
        index == experts[1:2, :], shares[1:2, :], 0.0
    )
    packet[me, n : n + 1, 0:channels] = jnp.sum(decay[...], axis=0, keepdims=True)
    greet(peers + lanes + [twin])
    notes = [
        go(packet.at[me], packet.at[me], small, d, peer) for d, peer in enumerate(peers)
    ]
    loads[0].wait()
    loads[1].wait()
    offsets = range(1, side)
    reach = side - 1
    first = {}
    for turn, (on_x, on_y) in enumerate([(all_b, all_a), (all_a, all_b)]):
        for d in offsets:
            base, at = 2 * turn * reach + d - 1, half(me)
            first["x", turn, d] = go(
                on_x.at[at], on_x.at[at], far, base, there(sp=place(0, d))
            )
            first["y", turn, d] = go(
                on_y.at[at], on_y.at[at], far, base + reach, there(sp=place(d, 0))
            )
    eye = lax.broadcasted_iota(jnp.int32, (rows, rows), 0) == lax.broadcasted_iota(
        jnp.int32, (rows, rows), 1
    )
    tile = 256 if units % 256 == 0 else 128
    own, other = ds(core * wide, wide), ds((1 - core) * wide, wide)

    def relay(copy, full, block, slot):
        copy.wait_recv()
        at = half(block)
        return go(full.at[at], full.at[at], near, slot, twin)

    def expert(block):
        at = whole(block)
        line = packet[block, pl.ds(me, 1), :]
        scale = jnp.sum(jnp.where(eye, line, 0.0), axis=1, keepdims=True)
        routed[at, :] = (all_b[at, :].astype(F32) * scale).astype(BF16)
        for start in range(0, units, tile):
            j = slice(start, start + tile)
            gate = dot(all_a[at, :], gate_w[:, j], NN, None)
            upper = dot(all_a[at, :], up_w[:, j], NN, None)
            d_hidden = dot(routed[at, :], down_w[j, :], NT, None)
            sigmoid_gate = jax.nn.sigmoid(gate)
            active = gate * sigmoid_gate
            hidden[at, j] = (active * upper).astype(BF16)
            d_upper[at, j] = (d_hidden * active).astype(BF16)
            d_gate[at, j] = (
                d_hidden * upper * sigmoid_gate * (1.0 + gate * (1.0 - sigmoid_gate))
            ).astype(BF16)

    def back(block, which):
        at = whole(block)
        for j in range(0, wide, 256):
            to = ds(which * wide + j, 256)
            slots[at, to] = (
                dot(d_gate[at, :], gate_w[to, :], NT, None)
                + dot(d_upper[at, :], up_w[to, :], NT, None)
            ).astype(BF16)

    crossing = {}

    def emit(dy, dx):
        block = place(dy, dx)
        slot = (dy % side) * side + dx % side
        expert(block)
        back(block, 1 - core)
        copy = go(slots.at[whole(block), other], got_t.at[slot], twin_s, slot, twin)
        back(block, core)
        copy.wait_recv()
        got_t[slot] = (
            slots[whole(block), own].astype(F32) + got_t[slot].astype(F32)
        ).astype(BF16)
        if slot:
            for h in range(2):
                cut = slice(h * part, (h + 1) * part)
                crossing[slot, h] = go(
                    got_t.at[slot, :, cut], got_p.at[slot - 1, :, cut], plane_s,
                    2 * (slot - 1) + h, there(sp=block),
                )

    for load in loads[2:5]:
        load.wait()
    emit(0, 0)
    second, passed = {}, {}
    flat = 4 * reach
    square = reach * reach
    for d in offsets:
        passed["y", 0, d] = relay(first["y", 0, d], all_a, place(-d, 0), reach + d - 1)
        at = half(place(-d, 0))
        for e in offsets:
            second[0, d, e] = go(
                all_a.at[at], all_a.at[at], far, flat + (d - 1) * reach + e - 1,
                there(sp=place(0, e)),
            )
        passed["x", 0, d] = relay(first["x", 0, d], all_b, place(0, -d), d - 1)
        at = half(place(0, -d))
        for e in offsets:
            second[1, e, d] = go(
                all_b.at[at], all_b.at[at], far, flat + square + (e - 1) * reach + d - 1,
                there(sp=place(e, 0)),
            )
    loads[5].wait()
    at = whole(me)
    shared = [
        go(all_s.at[at], all_s.at[at], small, n - 1 + d, peer)
        for d, peer in enumerate(peers)
    ]
    for d in offsets:
        passed["x", 1, d] = relay(first["x", 1, d], all_a, place(0, -d), 2 * reach + d - 1)
        passed["y", 1, d] = relay(first["y", 1, d], all_b, place(-d, 0), 3 * reach + d - 1)
    for note in notes:
        note.wait_recv()
    for d in offsets:
        for turn in range(2):
            passed["x", turn, d].wait_recv()
        emit(0, -d)
        for turn in range(2):
            passed["y", turn, d].wait_recv()
        emit(-d, 0)
    for d in offsets:
        for e in offsets:
            base = flat + (d - 1) * reach + e - 1
            pair = [
                relay(second[0, d, e], all_a, place(-d, -e), base),
                relay(second[1, d, e], all_b, place(-d, -e), base + square),
            ]
            for copy in pair:
                copy.wait_recv()
            emit(-d, -e)

    def gate_up(i, carry):
        at = ds(i * 256, 256)
        gate_o[0, at, :] = dot(all_a[:, at], d_gate[...], TN, None).astype(BF16)
        up_o[0, at, :] = dot(all_a[:, at], d_upper[...], TN, None).astype(BF16)
        return carry

    def down(i, carry):
        at = ds(i * 256, 256)
        down_o[0, :, at] = dot(hidden[...], routed[:, at], TN, None).astype(BF16)
        return carry

    steps = width // 256
    lax.fori_loop(0, steps // 2, gate_up, 0)
    third, fourth, fifth = {}, {}, []
    for h in range(2):
        cut = slice(h * part, (h + 1) * part)
        total = got_t[0, :, cut].astype(F32)
        for slot in range(1, n):
            crossing[slot, h].wait_recv()
            total = total + got_p[slot - 1, :, cut].astype(F32)
        sum_z[:, cut] = total.astype(BF16)
        for d in range(depth - 1):
            third[h, d] = go(
                sum_z.at[ds(along[d] * piece, piece), cut], got_z.at[d, :, cut], z_s,
                h * (depth - 1) + d, lanes[d],
            )
    lax.fori_loop(steps // 2, steps, gate_up, 0)
    kept = ds(z * piece, piece)
    for h in range(2):
        cut = slice(h * part, (h + 1) * part)
        to = ds(core * wide + h * part, part)
        total = all_b[ds(me * rows + z * piece, piece), to].astype(F32)
        total = total + sum_z[kept, cut].astype(F32)
        for d in range(depth - 1):
            third[h, d].wait_recv()
            total = total + got_z[d, :, cut].astype(F32)
        grad_in[kept, to] = total.astype(BF16)
        for d in range(depth - 1):
            fourth[h, d] = go(
                grad_in.at[kept, to], grad_in.at[kept, to], back_s,
                h * (depth - 1) + d, lanes[d],
            )
        fifth.append(
            go(grad_in.at[kept, to], grad_in.at[kept, to], twin_b, h * depth, twin)
        )
    lax.fori_loop(0, steps, down, 0)
    for h in range(2):
        to = ds(core * wide + h * part, part)
        for d in range(depth - 1):
            fourth[h, d].wait_recv()
            at = ds(lax.rem(z + depth - 1 - d, depth) * piece, piece)
            fifth.append(
                go(grad_in.at[at, to], grad_in.at[at, to], twin_b, h * depth + d + 1, twin)
            )
    for copy in shared + fifth:
        copy.wait_recv()
    for copy in started:
        copy.wait_send()


def mix_kernel(
    n, grad_in, out_proj, queries, log_decay, packet, mix_out, after, proj_in, starts, *sems
):
    me, lane = lax.axis_index("sp"), lax.axis_index("tp")
    core = lax.rem(lane, 2)
    twin = there(tp=lane + 1 - 2 * core)
    peers = [there(sp=lax.rem(me + d, n)) for d in range(1, n)]
    rows, width = grad_in.shape
    part = width // n
    split = rows // 2
    far, near, begin = (sems[2 * i : 2 * i + 2] for i in range(3))

    def ds(start, size):
        return pl.ds(pl.multiple_of(start, size), size)

    greet(peers + [twin])
    ours = []
    for d, peer in enumerate(peers):
        to = lax.rem(me + d + 1, n)
        ours.append(send(
            grad_in.at[ds(core * split, split), ds(to * part, part)],
            proj_in.at[ds(me * rows + core * split, split)], far, d, peer,
        ))
    proj_in[ds(me * rows, rows), :] = grad_in[:, ds(me * part, part)]
    mix = dot(grad_in[...], out_proj[...], NT, None)
    mix_out[...] = mix
    channels = queries.shape[1]
    heads = channels // DK
    wide = mix.shape[1] // heads
    lower = triangle(SPAN, False)
    ones = jnp.ones((SPAN, wide), F32)
    for h in range(heads):
        keyed = slice(h * DK, (h + 1) * DK)
        carry = None
        for n_ in reversed(range(rows // SPAN)):
            at = slice(n_ * SPAN, (n_ + 1) * SPAN)
            decay = log_decay[at, keyed]
            qd = queries[at, keyed].astype(F32) * jnp.exp(dot(lower, decay, NN))
            local = DK**-0.5 * dot(qd, mix[at, h * wide : (h + 1) * wide], TN)
            if carry is not None:
                local = local + jnp.exp(dot(decay, ones, TN)) * carry
            carry = local
        starts[me, keyed, :] = carry
    copies = [send(starts.at[me], starts.at[me], begin, d, peers[d]) for d in range(n - 1)]
    relayed = []
    for d in range(n - 1):
        ours[d].wait_recv()
        source = lax.rem(me + n - 1 - d, n)
        at = ds(source * rows + core * split, split)
        relayed.append(send(proj_in.at[at], proj_in.at[at], near, d, twin))
    index = lax.broadcasted_iota(jnp.int32, (n, channels), 0)
    decays = jnp.concatenate([packet[q, n : n + 1, 0:channels] for q in range(n)], axis=0)
    lanes = jnp.ones((n, wide), F32)
    total = jnp.zeros((channels, wide), F32)
    for d in range(n - 1):
        copies[d].wait_recv()
        source = lax.rem(me + n - 1 - d, n)
        passed = jnp.where((index > me) & (index < source), decays, 0.0)
        factor = jnp.exp(dot(passed, lanes, TN))
        total = total + jnp.where(source > me, factor, 0.0) * starts[source]
    after[...] = total
    for copy in relayed:
        copy.wait_recv()
    for copy in ours + copies + relayed:
        copy.wait_send()


def finish_kernel(queries, keys, values, log_decay, mix, state, after, dq_o, dk_o, dv_o, dl_o):
    rows, channels = queries.shape
    heads = channels // DK
    wide = values.shape[1] // heads
    lower = triangle(SPAN, False)
    upper = triangle(SPAN, True)
    ones = jnp.ones((SPAN, wide), F32)
    scale = DK**-0.5
    for h in range(heads):
        keyed = slice(h * DK, (h + 1) * DK)
        valued = slice(h * wide, (h + 1) * wide)
        g_end = after[keyed, :]
        for n in reversed(range(rows // SPAN)):
            at = slice(n * SPAN, (n + 1) * SPAN)
            q = queries[at, keyed].astype(F32)
            k = keys[at, keyed].astype(F32)
            v = values[at, valued].astype(F32)
            g = mix[at, valued]
            s0 = state[n, keyed, :]
            decay = log_decay[at, keyed]
            c = dot(lower, decay, NN)
            last = c[SPAN - 1 : SPAN, :]
            grow, shrink, to_end = jnp.exp(c), jnp.exp(-c), jnp.exp(last - c)
            qd, kd, ke = q * grow, k * shrink, k * to_end
            scores = dot(qd, kd, NT) * lower
            gv = dot(g, v, NT) * lower
            dq = scale * grow * (dot(gv, kd, NN) + dot(g, s0, NT))
            dk = scale * shrink * dot(gv, qd, TN) + to_end * dot(v, g_end, NT)
            dv = scale * dot(scores, g, TN) + dot(ke, g_end, NN)
            e_last = jnp.exp(dot(decay, ones, TN))
            s1 = e_last * s0 + dot(ke, v, TN)
            dq_o[at, keyed] = dq.astype(BF16)
            dk_o[at, keyed] = dk.astype(BF16)
            dv_o[at, valued] = dv.astype(BF16)
            dl_o[at, keyed] = dot(upper, q * dq - k * dk, NN) + dot(ones, s1 * g_end, NT)
            if n:
                g_end = DK**-0.5 * dot(qd, g, TN) + e_last * g_end


def last_kernel(
    gate, up, down, proj_in, all_s, queries, keys, values, log_decay, mix, state, after,
    gate_o, up_o, down_o, proj_o, dq_o, dk_o, dv_o, dl_o, sems,
):
    stores = [
        pltpu.make_async_copy(src, dst, sems.at[i])
        for i, (src, dst) in enumerate([(gate, gate_o), (up, up_o), (down, down_o)])
    ]
    for store in stores:
        store.start()
    proj_o[...] = dot(proj_in[...], all_s[...], TN, None)
    finish_kernel(
        queries, keys, values, log_decay, mix, state, after, dq_o, dk_o, dv_o, dl_o
    )
    for store in stores:
        store.wait()


def size_of(scratch):
    return sum(math.prod(s) * jnp.dtype(d).itemsize for s, d in scratch)


def call(kernel, outs, ins, args, scratch=(), sems=(), ident=None, flops=2 * 10**8):
    semaphores = [pltpu.SemaphoreType.DMA((count,)) for count in sems]
    limit = size_of(scratch) + (8 << 20)
    return pl.pallas_call(
        kernel,
        out_shape=[
            jax.ShapeDtypeStruct(s, d) if m == pl.ANY else m(s, d) for m, s, d in outs
        ],
        in_specs=[pl.BlockSpec(memory_space=m) for m in ins],
        out_specs=[pl.BlockSpec(memory_space=m) for m, s, d in outs],
        scratch_shapes=[pltpu.VMEM(s, d) for s, d in scratch] + semaphores,
        cost_estimate=pl.CostEstimate(flops=flops, bytes_accessed=10**6, transcendentals=0),
        compiler_params=pltpu.CompilerParams(
            collective_id=ident, has_side_effects=ident is not None, vmem_limit_bytes=limit
        ),
    )(*args)


def on_device(
    moe_input,
    cotangent,
    route_expert,
    route_weight,
    w_gate,
    w_up,
    w_down,
    out_proj,
    saved_out,
    queries,
    keys,
    values,
    log_decay,
    span_state,
):
    rows, width = moe_input.shape
    groups = lax.axis_size("sp")
    depth = lax.axis_size("tp") // 2
    units = w_gate.shape[2]
    tokens = groups * rows
    channels, wide = queries.shape[1], span_state.shape[2]
    lanes = values.shape[1]
    fast, slow = pltpu.VMEM, pl.ANY
    packet_rows = -(-(groups + 1) // 8) * 8
    reach = math.isqrt(groups) - 1
    links = 4 * reach + 2 * reach * reach

    def both(*counts):
        return [count for count in counts for _ in range(2)]

    grad_in, all_s, packet, gate_v, up_v, down_v = call(
        functools.partial(expert_kernel, groups, depth),
        [
            (fast, (rows, width), BF16),
            (fast, (tokens, lanes), BF16),
            (fast, (groups, packet_rows, rows), F32),
            (fast, w_gate.shape, BF16),
            (fast, w_up.shape, BF16),
            (fast, w_down.shape, BF16),
        ],
        [slow, slow, slow, fast, fast, fast, slow, slow, slow],
        (
            moe_input, cotangent, saved_out, route_expert.T, route_weight.T, log_decay,
            w_gate, w_up, w_down,
        ),
        scratch=[
            ((tokens, width), BF16),
            ((tokens, width), BF16),
            ((tokens, width), BF16),
            ((tokens, units), BF16),
            ((tokens, units), BF16),
            ((tokens, units), BF16),
            ((width, units), BF16),
            ((width, units), BF16),
            ((units, width), BF16),
            ((tokens, width), BF16),
            ((groups, rows, width // 2), BF16),
            ((groups - 1, rows, width // 2), BF16),
            ((rows, width // 2), BF16),
            ((depth - 1, rows // depth, width // 2), BF16),
        ],
        sems=[6] + both(
            links, links, 2 * (groups - 1), groups, 2 * (groups - 1), 2 * (depth - 1),
            2 * (depth - 1), 2 * depth,
        ),
        ident=1,
        flops=10**10,
    )
    mix, after, proj_in = call(
        functools.partial(mix_kernel, groups),
        [
            (fast, (rows, lanes), F32),
            (fast, (channels, wide), F32),
            (fast, (tokens, width // groups), BF16),
        ],
        [fast] * 5,
        (grad_in, out_proj, queries, log_decay, packet),
        scratch=[((groups, channels, wide), F32)],
        sems=both(groups - 1, groups - 1, groups - 1),
        ident=2,
    )
    return call(
        last_kernel,
        [
            (slow, w_gate.shape, BF16),
            (slow, w_up.shape, BF16),
            (slow, w_down.shape, BF16),
            (fast, (width // groups, lanes), F32),
            (fast, queries.shape, BF16),
            (fast, keys.shape, BF16),
            (fast, values.shape, BF16),
            (fast, log_decay.shape, F32),
        ],
        [fast] * 12,
        (
            gate_v, up_v, down_v, proj_in, all_s, queries, keys, values, log_decay, mix,
            span_state, after,
        ),
        sems=[3],
    )


def solution(mesh):
    placed = (
        P("sp", None),
        P("sp", None),
        P("sp", None),
        P("sp", None),
        P("sp", None, "tp"),
        P("sp", None, "tp"),
        P("sp", "tp", None),
        P("tp", None),
        P("sp", "tp"),
        P("sp", "tp"),
        P("sp", "tp"),
        P("sp", "tp"),
        P("sp", "tp"),
        P("sp", "tp", None),
    )
    return jax.shard_map(
        on_device,
        mesh=mesh,
        in_specs=placed,
        out_specs=(
            P("sp", None, "tp"),
            P("sp", None, "tp"),
            P("sp", "tp", None),
            P("sp", "tp"),
            P("sp", "tp"),
            P("sp", "tp"),
            P("sp", "tp"),
            P("sp", "tp"),
        ),
        check_vma=False,
    )
```

time: 135 us -> 87.2 us (0.65)
  Pallas kernels: 95.1 us -> 72 us
  matrix products: 14.4 us -> 0 us
  between operations: 14.2 us -> 0.73 us
  local copies, waits for them, and re-layouts: 2.55 us -> 14.1 us
  other arithmetic: 8.63 us -> 0 us
    pallas_call x5 -> x3, Pallas kernels: 95.1 us -> 72 us  [call(): pl.pallas_call(kernel, out_shape=[jax.ShapeDtypeStruct(s, d) if m == pl.A...]
    dot_general x6 -> x0, matrix products: 14.4 us -> none  [the longest x4 9.3 us: dot(): lax.dot_general(a, b, ((dims[0], dims[1]), ((), ())), precision=precision...]
    unnamed x18 -> x33, local copies, waits for them, and re-layouts: 1.84 us -> 14.1 us
    reduce_sum x4 -> x0, other arithmetic: 4.63 us -> none  [the longest x1 1.73 us: on_device(): after = jnp.sum(factor[:, :, None] * starts, axis=0)]
    convert_element_type x3 -> x0, other arithmetic: 3.93 us -> none  [the longest x1 2.14 us: on_device(): routed = (mine * cots.astype(F32)).astype(BF16)]
  transfers between devices with their start and end apart: 1 -> 0, of which waited for: 0 -> 0; matrix products, arithmetic and copies ran while one was open for 1% -> 0% of each run, Pallas kernels for 20% -> 0%
where the time goes in v1:
time: 87.2 us; the launch traced here: 86.8 us
  Pallas kernels  72 us (83%)
  local copies, waits for them, and re-layouts  14.1 us (16%)
    pallas_call x3, Pallas kernels, call(): pl.pallas_call(kernel, out_shape=[jax.ShapeDtypeStruct(s, d) if m == pl.A...  72 us
    unnamed x33, local copies, waits for them, and re-layouts  14.1 us

profile of v1, /device:TPU:0, one launch (start us, length us, event | category | flops | bytes accessed | tf_op | source)
XLA Modules:
  0.0 86.8 jit_solution(8495221390058983298)
XLA Ops:
  0.6 0.0 copy-start.1
  0.6 0.8 copy-done.1
  1.5 0.0 copy-start.6
  1.5 1.9 %copy-done.6 = bf16[1,2048,768]{2,1,0:T(8,128)(2,1)S(1)} copy-done((bf16[1,2048,768]{2,1,0:T(8,128)(2,1)S(1)}, bf16[1,2048,768]{2,1,0:T(8,128)(2,1)}, u32[]{:S(2)}) %copy-start.6) | copy-done | bytes 3145752
  3.4 0.0 copy-start.7
  3.4 1.9 %copy-done.7 = bf16[1,2048,768]{2,1,0:T(8,128)(2,1)S(1)} copy-done((bf16[1,2048,768]{2,1,0:T(8,128)(2,1)S(1)}, bf16[1,2048,768]{2,1,0:T(8,128)(2,1)}, u32[]{:S(2)}) %copy-start.7) | copy-done | bytes 3145752
  5.3 0.0 copy-start.8
  5.3 1.9 %copy-done.8 = bf16[1,768,2048]{2,1,0:T(8,128)(2,1)S(1)} copy-done((bf16[1,768,2048]{2,1,0:T(8,128)(2,1)S(1)}, bf16[1,768,2048]{2,1,0:T(8,128)(2,1)}, u32[]{:S(2)}) %copy-start.8) | copy-done | bytes 3145752
  7.1 0.0 copy-start.9
  7.2 1.0 %copy-done.9 = bf16[128,2048]{1,0:T(8,128)(2,1)S(1)} copy-done((bf16[128,2048]{1,0:T(8,128)(2,1)S(1)}, bf16[128,2048]{1,0:T(8,128)(2,1)}, u32[]{:S(2)}) %copy-start.9) | copy-done | bytes 524312
  8.2 0.0 copy-start.10
  8.2 1.0 %copy-done.10 = bf16[128,2048]{1,0:T(8,128)(2,1)S(1)} copy-done((bf16[128,2048]{1,0:T(8,128)(2,1)S(1)}, bf16[128,2048]{1,0:T(8,128)(2,1)}, u32[]{:S(2)}) %copy-start.10) | copy-done | bytes 524312
  9.2 0.0 copy-start.11
  9.2 0.8 copy-done.11
  10.1 0.0 copy-start.12
  10.1 0.7 copy-done.12
  10.8 0.0 copy-start.13
  10.8 0.7 copy-done.13
  11.4 0.0 copy-start.5
  11.5 55.1 %shard_map.197 = (bf16[128,2048]{1,0:T(8,128)(2,1)S(1)}, bf16[512,256]{1,0:T(8,128)(2,1)S(1)}, f32[4,8,128]{2,1,0:T(8,128)S(1)}, bf16[1,2048,768]{2,1,0:T(8,128)...) custom-call(bf16[128,2048]{1,0:T(8,128)(2,1)S(1)} %copy-done.9, ...), custom_call_target="tpu_custom_call" | custom-call | flops 10000000000 | bytes 1000000 | tf_op jit(solution)/shard_map/pallas_call | solution.py:447
  66.5 0.0 copy-done
  66.5 0.0 copy-done.3
  66.6 10.4 %shard_map.198 = (f32[128,256]{1,0:T(8,128)S(1)}, f32[128,128]{1,0:T(8,128)S(1)}, bf16[512,512]{1,0:T(8,128)(2,1)S(1)}) custom-call(bf16[128,2048]{1,0:T(8,128)(2,1)S(1)} %get-tuple-element.20.grad_in, bf16[256,2048]{1,0:T(8,128)(2,1)S(1)} %copy-done, bf16[128,128]{1,0:T(8,128)(2,1)S(1)} %copy-done.3, f32[128,128]{1,0:T(8,128)S(1)} %copy-done.1, ...), custom_call_target="tpu_custom_call" | custom-call | flops 200000000 | bytes 1000000 | tf_op jit(solution)/shard_map/pallas_call | solution.py:447
  77.0 0.0 copy-done.2
  77.0 0.0 copy-done.4
  77.0 0.0 copy-done.5
  77.0 6.4 %shard_map.199 = (bf16[1,2048,768]{2,1,0:T(8,128)(2,1)}, bf16[1,2048,768]{2,1,0:T(8,128)(2,1)}, bf16[1,768,2048]{2,1,0:T(8,128)(2,1)}, f32[512,256]{1,0:T(8,128)...) custom-call(bf16[1,2048,768]{2,1,0:T(8,128)(2,1)S(1)} %get-tuple-ele, ...), custom_call_target="tpu_custom_call" | custom-call | flops 200000000 | bytes 1000000 | tf_op jit(solution)/shard_map/pallas_call | solution.py:447
  83.5 0.6 copy.23
  84.1 0.6 copy.24
  84.7 0.6 copy.25
  85.4 0.6 copy.26
  86.0 0.8 copy.22
  (4 shorter events, 0.0 us)
Async XLA Ops:
  0.6 0.8 copy-start.1
  1.5 1.9 %copy-start.6 = (bf16[1,2048,768]{2,1,0:T(8,128)(2,1)S(1)}, bf16[1,2048,768]{2,1,0:T(8,128)(2,1)}, u32[]{:S(2)}) copy-start(bf16[1,2048,768]{2,1,0:T(8,128)(2,1)} %gate_h.1) | copy-start | bytes 9437188
  3.4 1.9 %copy-start.7 = (bf16[1,2048,768]{2,1,0:T(8,128)(2,1)S(1)}, bf16[1,2048,768]{2,1,0:T(8,128)(2,1)}, u32[]{:S(2)}) copy-start(bf16[1,2048,768]{2,1,0:T(8,128)(2,1)} %up_h.1) | copy-start | bytes 9437188
  5.3 1.9 %copy-start.8 = (bf16[1,768,2048]{2,1,0:T(8,128)(2,1)S(1)}, bf16[1,768,2048]{2,1,0:T(8,128)(2,1)}, u32[]{:S(2)}) copy-start(bf16[1,768,2048]{2,1,0:T(8,128)(2,1)} %down_h.1) | copy-start | bytes 9437188
  7.1 1.0 %copy-start.9 = (bf16[128,2048]{1,0:T(8,128)(2,1)S(1)}, bf16[128,2048]{1,0:T(8,128)(2,1)}, u32[]{:S(2)}) copy-start(bf16[128,2048]{1,0:T(8,128)(2,1)} %moe.1) | copy-start | bytes 1572868
  8.2 1.0 %copy-start.10 = (bf16[128,2048]{1,0:T(8,128)(2,1)S(1)}, bf16[128,2048]{1,0:T(8,128)(2,1)}, u32[]{:S(2)}) copy-start(bf16[128,2048]{1,0:T(8,128)(2,1)} %cot.1) | copy-start | bytes 1572868
  9.2 0.8 copy-start.11
  10.1 0.7 copy-start.12
  10.8 0.7 copy-start.13
  11.4 55.1 %copy-start = (bf16[256,2048]{1,0:T(8,128)(2,1)S(1)}, bf16[256,2048]{1,0:T(8,128)(2,1)}, u32[]{:S(2)}) copy-start(bf16[256,2048]{1,0:T(8,128)(2,1)} %out_proj.1) | copy-start | bytes 3145732
  11.4 55.1 %copy-start.3 = (bf16[128,128]{1,0:T(8,128)(2,1)S(1)}, bf16[128,128]{1,0:T(8,128)(2,1)}, u32[]{:S(2)}) copy-start(bf16[128,128]{1,0:T(8,128)(2,1)} %queries.3) | copy-start | bytes 98308
  11.4 65.6 %copy-start.2 = (f32[2,128,128]{2,1,0:T(8,128)S(1)}, f32[2,128,128]{2,1,0:T(8,128)}, u32[]{:S(2)}) copy-start(f32[2,128,128]{2,1,0:T(8,128)} %state.1) | copy-start | bytes 393220
  11.4 65.6 %copy-start.4 = (bf16[128,256]{1,0:T(8,128)(2,1)S(1)}, bf16[128,256]{1,0:T(8,128)(2,1)}, u32[]{:S(2)}) copy-start(bf16[128,256]{1,0:T(8,128)(2,1)} %values.1) | copy-start | bytes 196612
  11.4 65.6 %copy-start.5 = (bf16[128,128]{1,0:T(8,128)(2,1)S(1)}, bf16[128,128]{1,0:T(8,128)(2,1)}, u32[]{:S(2)}) copy-start(bf16[128,128]{1,0:T(8,128)(2,1)} %keys.1) | copy-start | bytes 98308

commit v2 on v1

v2 whole, which is shorter than its diff:
```python
import functools
import math

import jax
import jax.numpy as jnp
from jax import lax
from jax.experimental import pallas as pl
from jax.experimental.pallas import tpu as pltpu
from jax.sharding import PartitionSpec as P

DK = 64
SPAN = 64
CUTS = 2

HIGH = lax.Precision.HIGHEST
F32 = jnp.float32
BF16 = jnp.bfloat16


def dot(a, b, dims, precision=HIGH):
    return lax.dot_general(
        a, b, ((dims[0], dims[1]), ((), ())), precision=precision, preferred_element_type=F32
    )


NN = ((1,), (0,))
NT = ((1,), (1,))
TN = ((0,), (0,))


def triangle(size, upper):
    row = lax.broadcasted_iota(jnp.int32, (size, size), 0)
    col = lax.broadcasted_iota(jnp.int32, (size, size), 1)
    return ((row <= col) if upper else (row >= col)).astype(F32)


def there(sp=None, tp=None):
    where = {}
    if sp is not None:
        where["sp"] = sp
    if tp is not None:
        where["tp"] = tp
    return where


def greet(partners):
    barrier = pltpu.get_barrier_semaphore()
    for partner in partners:
        pl.semaphore_signal(
            barrier, inc=1, device_id=partner, device_id_type=pl.DeviceIdType.MESH
        )
    pl.semaphore_wait(barrier, len(partners))


def send(src, dst, sems, slot, partner):
    copy = pltpu.make_async_remote_copy(
        src_ref=src,
        dst_ref=dst,
        send_sem=sems[0].at[slot],
        recv_sem=sems[1].at[slot],
        device_id=partner,
        device_id_type=pl.DeviceIdType.MESH,
    )
    copy.start()
    return copy


def expert_kernel(
    n, depth, moe, cot, saved, experts_h, shares_h, decay_h, gate_h, up_h, down_h,
    out_h, query_h, key_h, value_h, state_h,
    gate_o, up_o, down_o, all_s, proj_in, after, mid, fall, ends, to_end, ke, dq_o, dk_o, dv_o,
    grad_in, packet, out_proj, queries, keys, values, state, starts, factors,
    grow, shrink, qd, kd, scores,
    all_a, all_b, routed, hidden, d_gate, d_upper, gate_w, up_w,
    gate_t, up_t, down_t,
    slots, mine, got_t, got_p, sum_z, got_z, experts, shares, decay, local, *sems,
):
    me, lane = lax.axis_index("sp"), lax.axis_index("tp")
    core, z = lax.rem(lane, 2), lax.div(lane, 2)
    side = math.isqrt(n)
    y, x = lax.div(me, side), lax.rem(me, side)
    rows, width = moe.shape
    units = hidden.shape[1]
    channels = decay.shape[1]
    split = rows // 2
    wide = width // 2
    cuts = CUTS
    part = wide // cuts
    piece = rows // depth
    far, near, small, twin_s, plane_s, z_s, back_s, twin_b, slice_s, slice_t, begin = (
        sems[2 * i : 2 * i + 2] for i in range(11)
    )

    def ds(start, size):
        return pl.ds(pl.multiple_of(start, size), size)

    def place(dy, dx):
        return lax.rem(y + dy + side, side) * side + lax.rem(x + dx + side, side)

    def half(block):
        return ds(block * rows + core * split, split)

    def whole(block):
        return ds(block * rows, rows)

    started = []

    def go(*args):
        copy = send(*args)
        started.append(copy)
        return copy

    twin = there(tp=lane + 1 - 2 * core)
    peers = [there(sp=lax.rem(me + d, n)) for d in range(1, n)]
    along = [lax.rem(z + d, depth) for d in range(1, depth)]
    lanes = [there(tp=2 * far_z + core) for far_z in along]
    loads = [
        pltpu.make_async_copy(src, dst, local.at[i])
        for i, (src, dst) in enumerate([
            (moe, all_a.at[whole(me)]),
            (cot, all_b.at[whole(me)]),
            (gate_h.at[0], gate_w),
            (up_h.at[0], up_w),
            (down_h.at[0], down_o.at[0]),
            (saved, all_s.at[whole(me)]),
            (experts_h, experts),
            (shares_h, shares),
            (decay_h, decay),
            (query_h, queries),
            (key_h, keys),
            (value_h, values),
            (state_h, state),
            (out_h, out_proj),
        ])
    ]
    for load in loads[6:9] + loads[:6] + loads[9:]:
        load.start()
    for load in loads[6:9]:
        load.wait()
    index = lax.broadcasted_iota(jnp.int32, (n, rows), 0)
    packet[me, 0:n, :] = jnp.where(index == experts[0:1, :], shares[0:1, :], 0.0) + jnp.where(
        index == experts[1:2, :], shares[1:2, :], 0.0
    )
    packet[me, n : n + 1, 0:channels] = jnp.sum(decay[...], axis=0, keepdims=True)
    greet(peers + lanes + [twin])
    notes = [
        go(packet.at[me], packet.at[me], small, d, peer) for d, peer in enumerate(peers)
    ]
    loads[0].wait()
    loads[1].wait()
    offsets = range(1, side)
    reach = side - 1
    first = {}
    for turn, (on_x, on_y) in enumerate([(all_b, all_a), (all_a, all_b)]):
        for d in offsets:
            base, at = 2 * turn * reach + d - 1, half(me)
            first["x", turn, d] = go(
                on_x.at[at], on_x.at[at], far, base, there(sp=place(0, d))
            )
            first["y", turn, d] = go(
                on_y.at[at], on_y.at[at], far, base + reach, there(sp=place(d, 0))
            )
    eye = lax.broadcasted_iota(jnp.int32, (rows, rows), 0) == lax.broadcasted_iota(
        jnp.int32, (rows, rows), 1
    )
    tile = 256 if units % 256 == 0 else 128

    def relay(copy, full, block, slot):
        copy.wait_recv()
        at = half(block)
        return go(full.at[at], full.at[at], near, slot, twin)

    def turn_over(src, dst):
        columns = src.shape[1]
        strip = 256 if columns % 256 == 0 else 128

        def step(i, carry):
            at = ds(i * 256, 256)
            for j in range(0, columns, strip):
                dst[j : j + strip, at] = src[at, j : j + strip].T
            return carry

        lax.fori_loop(0, src.shape[0] // 256, step, 0)

    def rows_of(ref, blocks):
        parts = [ref[whole(block), :] for block in blocks]
        return parts[0] if len(parts) == 1 else jnp.concatenate(parts, axis=0)

    def expert(blocks):
        for block in blocks:
            at = whole(block)
            line = packet[block, pl.ds(me, 1), :]
            scale = jnp.sum(jnp.where(eye, line, 0.0), axis=1, keepdims=True)
            routed[at, :] = (all_b[at, :].astype(F32) * scale).astype(BF16)
        for start in range(0, units, tile):
            j = slice(start, start + tile)
            gate = dot(rows_of(all_a, blocks), gate_w[:, j], NN, None)
            upper = dot(rows_of(all_a, blocks), up_w[:, j], NN, None)
            d_hidden = dot(rows_of(routed, blocks), down_t[:, j], NN, None)
            sigmoid_gate = jax.nn.sigmoid(gate)
            active = gate * sigmoid_gate
            made = [
                (hidden, active * upper),
                (d_upper, d_hidden * active),
                (
                    d_gate,
                    d_hidden * upper * sigmoid_gate * (1.0 + gate * (1.0 - sigmoid_gate)),
                ),
            ]
            for ref, value in made:
                for i, block in enumerate(blocks):
                    ref[whole(block), j] = value[i * rows : (i + 1) * rows].astype(BF16)

    def back(blocks, which):
        for j in range(0, wide, 256):
            to = ds(which * wide + j, 256)
            value = dot(rows_of(d_gate, blocks), gate_t[:, to], NN, None) + dot(
                rows_of(d_upper, blocks), up_t[:, to], NN, None
            )
            yield slice(j, j + 256), value

    wide_v = values.shape[1]
    heads = channels // DK
    value_dim = wide_v // heads
    spans = rows // SPAN
    row = lax.broadcasted_iota(jnp.int32, (rows, rows), 0)
    col = lax.broadcasted_iota(jnp.int32, (rows, rows), 1)
    causal = (row >= col) & (lax.div(row, SPAN) == lax.div(col, SPAN))

    def keyed(h):
        return slice(h * DK, (h + 1) * DK)

    def valued(h):
        return slice(h * value_dim, (h + 1) * value_dim)

    def span(i):
        return slice(i * SPAN, (i + 1) * SPAN)

    def prepare():
        c = dot(causal.astype(F32), decay[...], NN)
        ones = jnp.ones((SPAN, value_dim), F32)
        grow[...] = jnp.exp(c)
        shrink[...] = jnp.exp(-c)
        for i in range(spans):
            at = span(i)
            last = c[(i + 1) * SPAN - 1 : (i + 1) * SPAN, :]
            to_end[at, :] = jnp.exp(last - c[at, :])
            fall[i] = jnp.exp(dot(decay[at, :], ones, TN))
        qd[...] = (queries[...].astype(F32) * grow[...]).astype(BF16)
        kd[...] = (keys[...].astype(F32) * shrink[...]).astype(BF16)
        ke[...] = (keys[...].astype(F32) * to_end[...]).astype(BF16)
        for h in range(heads):
            scores[h] = jnp.where(
                causal, dot(qd[:, keyed(h)], kd[:, keyed(h)], NT, None), 0.0
            ).astype(BF16)
            for i in range(spans):
                ends[i, keyed(h), :] = fall[i, keyed(h), :] * state[i, keyed(h), :] + dot(
                    ke[span(i), keyed(h)], values[span(i), valued(h)], TN, None
                )

    crossing = {}

    def emit(*steps):
        blocks = [place(dy, dx) for dy, dx in steps]
        marks = [(dy % side) * side + dx % side for dy, dx in steps]
        expert(blocks)
        for cut, value in back(blocks, 1 - core):
            for i, block in enumerate(blocks):
                slots[whole(block), cut] = value[i * rows : (i + 1) * rows].astype(BF16)
        swaps = [
            go(slots.at[whole(block)], got_t.at[slot], twin_s, slot, twin)
            for block, slot in zip(blocks, marks)
        ]
        for cut, value in back(blocks, core):
            mine[0 : len(blocks) * rows, cut] = value
        for i, (block, slot, copy) in enumerate(zip(blocks, marks, swaps)):
            copy.wait_recv()
            got_t[slot] = (
                mine[i * rows : (i + 1) * rows, :] + got_t[slot].astype(F32)
            ).astype(BF16)
            for h in range(cuts if slot else 0):
                cut = slice(h * part, (h + 1) * part)
                crossing[slot, h] = go(
                    got_t.at[slot, :, cut], got_p.at[slot - 1, :, cut], plane_s,
                    cuts * (slot - 1) + h, there(sp=block),
                )

    for load in loads[9:]:
        load.wait()
    prepare()
    for load in loads[2:5]:
        load.wait()
    turn_over(down_o.at[0], down_t)
    turn_over(gate_w, gate_t)
    turn_over(up_w, up_t)
    second, passed = {}, {}
    flat = 4 * reach
    square = reach * reach
    for d in offsets:
        passed["y", 0, d] = relay(first["y", 0, d], all_a, place(-d, 0), reach + d - 1)
        at = half(place(-d, 0))
        for e in offsets:
            second[0, d, e] = go(
                all_a.at[at], all_a.at[at], far, flat + (d - 1) * reach + e - 1,
                there(sp=place(0, e)),
            )
        passed["x", 0, d] = relay(first["x", 0, d], all_b, place(0, -d), d - 1)
        at = half(place(0, -d))
        for e in offsets:
            second[1, e, d] = go(
                all_b.at[at], all_b.at[at], far, flat + square + (e - 1) * reach + d - 1,
                there(sp=place(e, 0)),
            )
    emit((0, 0))
    for d in offsets:
        passed["x", 1, d] = relay(first["x", 1, d], all_a, place(0, -d), 2 * reach + d - 1)
        passed["y", 1, d] = relay(first["y", 1, d], all_b, place(-d, 0), 3 * reach + d - 1)
    for note in notes:
        note.wait_recv()
    order = lax.broadcasted_iota(jnp.int32, (n, channels), 0)
    decays = jnp.concatenate([packet[q, n : n + 1, 0:channels] for q in range(n)], axis=0)
    for d in range(n - 1):
        source = lax.rem(me + n - 1 - d, n)
        between = jnp.where((order > me) & (order < source), decays, 0.0)
        factor = jnp.exp(dot(between, jnp.ones((n, value_dim), F32), TN))
        factors[d] = jnp.where(source > me, factor, 0.0)
    for d in offsets:
        for turn in range(2):
            passed["x", turn, d].wait_recv()
            passed["y", turn, d].wait_recv()
        emit((0, -d), (-d, 0))
    for d in offsets:
        for e in offsets:
            base = flat + (d - 1) * reach + e - 1
            pair = [
                relay(second[0, d, e], all_a, place(-d, -e), base),
                relay(second[1, d, e], all_b, place(-d, -e), base + square),
            ]
            for copy in pair:
                copy.wait_recv()
            emit((-d, -e))

    def gate_up(i, carry):
        at = ds(i * 256, 256)
        gate_o[0, at, :] = dot(all_a[:, at], d_gate[...], TN, None).astype(BF16)
        up_o[0, at, :] = dot(all_a[:, at], d_upper[...], TN, None).astype(BF16)
        return carry

    def down(i, carry):
        at = ds(i * tile, tile)
        turned = hidden[:, at].T
        for j in range(0, width, 512):
            to = slice(j, j + 512)
            down_o[0, at, to] = dot(turned, routed[:, to], NN, None).astype(BF16)
        return carry

    steps = width // 256
    turns = units // tile
    lax.fori_loop(0, steps, gate_up, 0)
    third, fourth, fifth = {}, {}, []
    for h in range(cuts):
        cut = slice(h * part, (h + 1) * part)
        total = got_t[0, :, cut].astype(F32)
        for slot in range(1, n):
            crossing[slot, h].wait_recv()
            total = total + got_p[slot - 1, :, cut].astype(F32)
        sum_z[:, cut] = total.astype(BF16)
        for d in range(depth - 1):
            third[h, d] = go(
                sum_z.at[ds(along[d] * piece, piece), cut], got_z.at[d, :, cut], z_s,
                h * (depth - 1) + d, lanes[d],
            )
    loads[5].wait()
    at = whole(me)
    shared = [
        go(all_s.at[at], all_s.at[at], small, n - 1 + d, peer)
        for d, peer in enumerate(peers)
    ]
    lax.fori_loop(0, turns // 2, down, 0)
    kept = ds(z * piece, piece)
    for h in range(cuts):
        cut = slice(h * part, (h + 1) * part)
        to = ds(core * wide + h * part, part)
        total = all_b[ds(me * rows + z * piece, piece), to].astype(F32)
        total = total + sum_z[kept, cut].astype(F32)
        for d in range(depth - 1):
            third[h, d].wait_recv()
            total = total + got_z[d, :, cut].astype(F32)
        grad_in[kept, to] = total.astype(BF16)
        for d in range(depth - 1):
            fourth[h, d] = go(
                grad_in.at[kept, to], grad_in.at[kept, to], back_s,
                h * (depth - 1) + d, lanes[d],
            )
        fifth.append(
            go(grad_in.at[kept, to], grad_in.at[kept, to], twin_b, h * depth, twin)
        )
    lax.fori_loop(turns // 2, turns, down, 0)
    for h in range(cuts):
        to = ds(core * wide + h * part, part)
        for d in range(depth - 1):
            fourth[h, d].wait_recv()
            at = ds(lax.rem(z + depth - 1 - d, depth) * piece, piece)
            fifth.append(
                go(grad_in.at[at, to], grad_in.at[at, to], twin_b, h * depth + d + 1, twin)
            )
    for copy in fifth:
        copy.wait_recv()
    slab = width // n
    mix = dot(grad_in[...], out_proj[...], NT, None)
    g = mix.astype(BF16)
    scale = DK**-0.5
    for h in range(heads):
        carry = None
        for i in reversed(range(spans)):
            local_g = scale * dot(qd[span(i), keyed(h)], g[span(i), valued(h)], TN, None)
            mid[i, keyed(h), :] = local_g
            carry = local_g if carry is None else local_g + fall[i, keyed(h), :] * carry
        starts[me, keyed(h), :] = carry.astype(BF16)
    opened = [go(starts.at[me], starts.at[me], begin, d, peers[d]) for d in range(n - 1)]
    sliced = [
        go(
            grad_in.at[ds(core * split, split), ds(lax.rem(me + d + 1, n) * slab, slab)],
            proj_in.at[half(me)], slice_s, d, peer,
        )
        for d, peer in enumerate(peers)
    ]
    proj_in[whole(me), :] = grad_in[:, ds(me * slab, slab)]
    for h in range(heads):
        gh = g[:, valued(h)]
        gv = jnp.where(causal, dot(gh, values[:, valued(h)], NT, None), 0.0).astype(BF16)
        past = jnp.concatenate([
            dot(gh[span(i), :], state[i, keyed(h), :].astype(BF16), NT, None)
            for i in range(spans)
        ], axis=0)
        dq_o[:, keyed(h)] = scale * grow[:, keyed(h)] * (
            dot(gv, kd[:, keyed(h)], NN, None) + past
        )
        dk_o[:, keyed(h)] = scale * shrink[:, keyed(h)] * dot(gv, qd[:, keyed(h)], TN, None)
        dv_o[:, valued(h)] = scale * dot(scores[h], gh, TN, None)
    total = jnp.zeros((channels, value_dim), F32)
    for d in range(n - 1):
        opened[d].wait_recv()
        total = total + factors[d] * starts[lax.rem(me + n - 1 - d, n)].astype(F32)
    after[...] = total
    relayed = []
    for d in range(n - 1):
        sliced[d].wait_recv()
        at = half(lax.rem(me + n - 1 - d, n))
        relayed.append(go(proj_in.at[at], proj_in.at[at], slice_t, d, twin))
    for copy in shared + relayed:
        copy.wait_recv()
    for copy in started:
        copy.wait_send()


def last_kernel(
    gate, up, down, all_s, proj_in, after, mid, fall, ends, to_end, ke, dq, dk_p, dv_p,
    queries, keys, values,
    gate_o, up_o, down_o, proj_o, dq_o, dk_o, dv_o, dl_o,
    proj_v, dq_v, dk_v, dv_v, dl_v, sems,
):
    stores = []

    def store(src, dst):
        copy = pltpu.make_async_copy(src, dst, sems.at[len(stores)])
        copy.start()
        stores.append(copy)

    for src, dst in [(gate, gate_o), (up, up_o), (down, down_o)]:
        store(src, dst)
    dq_v[...] = dq[...].astype(BF16)
    store(dq_v, dq_o)
    rows, channels = queries.shape
    heads = channels // DK
    wide = values.shape[1] // heads
    ones = jnp.ones((SPAN, wide), F32)
    upper = triangle(SPAN, True)
    g_end = after[...]
    for n in reversed(range(rows // SPAN)):
        at = slice(n * SPAN, (n + 1) * SPAN)
        narrow = g_end.astype(BF16)
        grown = ends[n] * g_end
        for h in range(heads):
            keyed = slice(h * DK, (h + 1) * DK)
            valued = slice(h * wide, (h + 1) * wide)
            dk = dk_p[at, keyed] + to_end[at, keyed] * dot(
                values[at, valued], narrow[keyed, :], NT, None
            )
            dv = dv_p[at, valued] + dot(ke[at, keyed], narrow[keyed, :], NN, None)
            dk_v[at, keyed] = dk.astype(BF16)
            dv_v[at, valued] = dv.astype(BF16)
            moved = queries[at, keyed].astype(F32) * dq[at, keyed] - keys[at, keyed].astype(
                F32
            ) * dk
            dl_v[at, keyed] = dot(upper, moved, NN) + dot(ones, grown[keyed, :], NT)
        if n:
            g_end = mid[n] + fall[n] * g_end
    for src, dst in [(dk_v, dk_o), (dv_v, dv_o), (dl_v, dl_o)]:
        store(src, dst)
    proj_v[...] = dot(proj_in[...], all_s[...], TN, None)
    store(proj_v, proj_o)
    for copy in stores:
        copy.wait()


def size_of(scratch):
    return sum(math.prod(s) * jnp.dtype(d).itemsize for s, d in scratch)


def call(kernel, outs, ins, args, scratch=(), sems=(), ident=None, flops=2 * 10**8):
    semaphores = [pltpu.SemaphoreType.DMA((count,)) for count in sems]
    limit = size_of(scratch) + (4 << 20)
    return pl.pallas_call(
        kernel,
        out_shape=[m(s, d) for m, s, d in outs],
        in_specs=[pl.BlockSpec(memory_space=m) for m in ins],
        out_specs=[pl.BlockSpec(memory_space=m) for m, s, d in outs],
        scratch_shapes=[pltpu.VMEM(s, d) for s, d in scratch] + semaphores,
        cost_estimate=pl.CostEstimate(flops=flops, bytes_accessed=10**6, transcendentals=0),
        compiler_params=pltpu.CompilerParams(
            collective_id=ident, has_side_effects=ident is not None, vmem_limit_bytes=limit
        ),
    )(*[
        pltpu.with_memory_space_constraint(a, m) if m == pltpu.HBM else a
        for m, a in zip(ins, args)
    ])


def on_device(
    moe_input,
    cotangent,
    route_expert,
    route_weight,
    w_gate,
    w_up,
    w_down,
    out_proj,
    saved_out,
    queries,
    keys,
    values,
    log_decay,
    span_state,
):
    rows, width = moe_input.shape
    groups = lax.axis_size("sp")
    depth = lax.axis_size("tp") // 2
    units = w_gate.shape[2]
    tokens = groups * rows
    channels, wide = queries.shape[1], span_state.shape[2]
    lanes = values.shape[1]
    fast, slow = pltpu.VMEM, pltpu.HBM
    packet_rows = -(-(groups + 1) // 8) * 8
    reach = math.isqrt(groups) - 1
    links = 4 * reach + 2 * reach * reach

    def both(*counts):
        return [count for count in counts for _ in range(2)]

    spans = rows // SPAN
    heads = channels // DK
    made = call(
        functools.partial(expert_kernel, groups, depth),
        [
            (fast, w_gate.shape, BF16),
            (fast, w_up.shape, BF16),
            (fast, w_down.shape, BF16),
            (fast, (tokens, lanes), BF16),
            (fast, (tokens, width // groups), BF16),
            (fast, (channels, wide), F32),
            (fast, (spans, channels, wide), F32),
            (fast, (spans, channels, wide), F32),
            (fast, (spans, channels, wide), F32),
            (fast, (rows, channels), F32),
            (fast, (rows, channels), BF16),
            (fast, (rows, channels), F32),
            (fast, (rows, channels), F32),
            (fast, (rows, lanes), F32),
        ],
        [slow] * 14,
        (
            moe_input, cotangent, saved_out, route_expert.T, route_weight.T, log_decay,
            w_gate, w_up, w_down, out_proj, queries, keys, values, span_state,
        ),
        scratch=[
            ((rows, width), BF16),
            ((groups, packet_rows, rows), F32),
            (out_proj.shape, BF16),
            (queries.shape, BF16),
            (keys.shape, BF16),
            (values.shape, BF16),
            (span_state.shape, F32),
            ((groups, channels, wide), BF16),
            ((groups - 1, channels, wide), F32),
            ((rows, channels), F32),
            ((rows, channels), F32),
            ((rows, channels), BF16),
            ((rows, channels), BF16),
            ((heads, rows, rows), BF16),
            ((tokens, width), BF16),
            ((tokens, width), BF16),
            ((tokens, width), BF16),
            ((tokens, units), BF16),
            ((tokens, units), BF16),
            ((tokens, units), BF16),
            ((width, units), BF16),
            ((width, units), BF16),
            ((units, width), BF16),
            ((units, width), BF16),
            ((width, units), BF16),
            ((tokens, width // 2), BF16),
            ((2 * rows, width // 2), F32),
            ((groups, rows, width // 2), BF16),
            ((groups - 1, rows, width // 2), BF16),
            ((rows, width // 2), BF16),
            ((depth - 1, rows // depth, width // 2), BF16),
            ((2, rows), jnp.int32),
            ((2, rows), F32),
            (log_decay.shape, F32),
        ],
        sems=[14] + both(
            links, links, 2 * (groups - 1), groups, CUTS * (groups - 1), CUTS * (depth - 1),
            CUTS * (depth - 1), CUTS * depth, groups - 1, groups - 1, groups - 1,
        ),
        ident=1,
        flops=10**10,
    )
    small = [
        ((width // groups, lanes), F32),
        (queries.shape, BF16),
        (keys.shape, BF16),
        (values.shape, BF16),
        (log_decay.shape, F32),
    ]
    return call(
        last_kernel,
        [
            (slow, w_gate.shape, BF16),
            (slow, w_up.shape, BF16),
            (slow, w_down.shape, BF16),
            *((slow, s, d) for s, d in small),
        ],
        [fast] * 17,
        (*made, queries, keys, values),
        scratch=small,
        sems=[8],
    )


def solution(mesh):
    placed = (
        P("sp", None),
        P("sp", None),
        P("sp", None),
        P("sp", None),
        P("sp", None, "tp"),
        P("sp", None, "tp"),
        P("sp", "tp", None),
        P("tp", None),
        P("sp", "tp"),
        P("sp", "tp"),
        P("sp", "tp"),
        P("sp", "tp"),
        P("sp", "tp"),
        P("sp", "tp", None),
    )
    return jax.shard_map(
        on_device,
        mesh=mesh,
        in_specs=placed,
        out_specs=(
            P("sp", None, "tp"),
            P("sp", None, "tp"),
            P("sp", "tp", None),
            P("sp", "tp"),
            P("sp", "tp"),
            P("sp", "tp"),
            P("sp", "tp"),
            P("sp", "tp"),
        ),
        check_vma=False,
    )
```

time: 87.2 us -> 66.4 us (0.76)
  local copies, waits for them, and re-layouts: 14.1 us -> 0.01 us
  Pallas kernels: 72 us -> 65.5 us
    unnamed x33 -> x6, local copies, waits for them, and re-layouts: 14.1 us -> 0.01 us
    pallas_call x3 -> x2, Pallas kernels: 72 us -> 65.5 us  [call(): pl.pallas_call(kernel, out_shape=[m(s, d) for m, s, d in outs], in_specs=...]
where the time goes in v2:
time: 66.4 us; the launch traced here: 66.2 us
  Pallas kernels  65.5 us (99%)
  between operations  0.69 us (1%)
    pallas_call x2, Pallas kernels, call(): pl.pallas_call(kernel, out_shape=[m(s, d) for m, s, d in outs], in_specs=...  65.5 us

profile of v2, /device:TPU:0, one launch (start us, length us, event | category | flops | bytes accessed | tf_op | source)
XLA Modules:
  0.0 66.2 jit_solution(5503861210114433434)
XLA Ops:
  0.6 0.0 copy-start
  0.6 0.0 copy-start.1
  0.7 0.0 copy-start.2
  0.7 61.0 %shard_map.197 = (bf16[1,2048,768]{2,1,0:T(8,128)(2,1)S(1)}, bf16[1,2048,768]{2,1,0:T(8,128)(2,1)S(1)}, bf16[1,768,2048]{2,1,0:T(8,128)(2,1)S(1)}, bf16[512,256]...) custom-call(bf16[128,2048]{1,0:T(8,128)(2,1)} %moe.1, ...), custom_call_target="tpu_custom_call" | custom-call | flops 10000000000 | bytes 1000000 | tf_op jit(solution)/shard_map/pallas_call | solution.py:514
  61.7 0.0 copy-done
  61.7 0.0 copy-done.1
  61.7 0.0 copy-done.2
  61.7 4.5 %shard_map.198 = (bf16[1,2048,768]{2,1,0:T(8,128)(2,1)}, bf16[1,2048,768]{2,1,0:T(8,128)(2,1)}, bf16[1,768,2048]{2,1,0:T(8,128)(2,1)}, f32[512,256]{1,0:T(8,128)...) custom-call(bf16[1,2048,768]{2,1,0:T(8,128)(2,1)S(1)} %get-tuple-element., ...), custom_call_target="tpu_custom_call" | custom-call | flops 200000000 | bytes 1000000 | tf_op jit(solution)/shard_map/pallas_call | solution.py:514
Async XLA Ops:
  0.6 61.0 %copy-start = (bf16[128,256]{1,0:T(8,128)(2,1)S(1)}, bf16[128,256]{1,0:T(8,128)(2,1)}, u32[]{:S(2)}) copy-start(bf16[128,256]{1,0:T(8,128)(2,1)} %values.1) | copy-start | bytes 196612
  0.6 61.0 %copy-start.1 = (bf16[128,128]{1,0:T(8,128)(2,1)S(1)}, bf16[128,128]{1,0:T(8,128)(2,1)}, u32[]{:S(2)}) copy-start(bf16[128,128]{1,0:T(8,128)(2,1)} %queries.1) | copy-start | bytes 98308
  0.7 61.0 %copy-start.2 = (bf16[128,128]{1,0:T(8,128)(2,1)S(1)}, bf16[128,128]{1,0:T(8,128)(2,1)}, u32[]{:S(2)}) copy-start(bf16[128,128]{1,0:T(8,128)(2,1)} %keys.1) | copy-start | bytes 98308

commit v3 on v2

--- a/solution.py
+++ b/solution.py
@@ -133,8 +133,26 @@
             (out_h, out_proj),
         ])
     ]
-    for load in loads[6:9] + loads[:6] + loads[9:]:
+    for load in loads[:2] + loads[6:9] + loads[2:6] + loads[9:]:
         load.start()
+    greet(peers + lanes + [twin])
+    loads[0].wait()
+    loads[1].wait()
+    offsets = range(1, side)
+    reach = side - 1
+    first = {}
+
+    def spread(turn, on_x, on_y):
+        for d in offsets:
+            base, at = 2 * turn * reach + d - 1, half(me)
+            first["x", turn, d] = go(
+                on_x.at[at], on_x.at[at], far, base, there(sp=place(0, d))
+            )
+            first["y", turn, d] = go(
+                on_y.at[at], on_y.at[at], far, base + reach, there(sp=place(d, 0))
+            )
+
+    spread(0, all_b, all_a)
     for load in loads[6:9]:
         load.wait()
     index = lax.broadcasted_iota(jnp.int32, (n, rows), 0)
@@ -142,24 +160,10 @@
         index == experts[1:2, :], shares[1:2, :], 0.0
     )
     packet[me, n : n + 1, 0:channels] = jnp.sum(decay[...], axis=0, keepdims=True)
-    greet(peers + lanes + [twin])
     notes = [
         go(packet.at[me], packet.at[me], small, d, peer) for d, peer in enumerate(peers)
     ]
-    loads[0].wait()
-    loads[1].wait()
-    offsets = range(1, side)
-    reach = side - 1
-    first = {}
-    for turn, (on_x, on_y) in enumerate([(all_b, all_a), (all_a, all_b)]):
-        for d in offsets:
-            base, at = 2 * turn * reach + d - 1, half(me)
-            first["x", turn, d] = go(
-                on_x.at[at], on_x.at[at], far, base, there(sp=place(0, d))
-            )
-            first["y", turn, d] = go(
-                on_y.at[at], on_y.at[at], far, base + reach, there(sp=place(d, 0))
-            )
+    spread(1, all_a, all_b)
     eye = lax.broadcasted_iota(jnp.int32, (rows, rows), 0) == lax.broadcasted_iota(
         jnp.int32, (rows, rows), 1
     )
@@ -211,8 +215,8 @@
                 for i, block in enumerate(blocks):
                     ref[whole(block), j] = value[i * rows : (i + 1) * rows].astype(BF16)
 
-    def back(blocks, which):
-        for j in range(0, wide, 256):
+    def back(blocks, which, h):
+        for j in range(h * part, (h + 1) * part, 256):
             to = ds(which * wide + j, 256)
             value = dot(rows_of(d_gate, blocks), gate_t[:, to], NN, None) + dot(
                 rows_of(d_upper, blocks), up_t[:, to], NN, None
@@ -264,26 +268,31 @@
         blocks = [place(dy, dx) for dy, dx in steps]
         marks = [(dy % side) * side + dx % side for dy, dx in steps]
         expert(blocks)
-        for cut, value in back(blocks, 1 - core):
-            for i, block in enumerate(blocks):
-                slots[whole(block), cut] = value[i * rows : (i + 1) * rows].astype(BF16)
-        swaps = [
-            go(slots.at[whole(block)], got_t.at[slot], twin_s, slot, twin)
-            for block, slot in zip(blocks, marks)
-        ]
-        for cut, value in back(blocks, core):
-            mine[0 : len(blocks) * rows, cut] = value
-        for i, (block, slot, copy) in enumerate(zip(blocks, marks, swaps)):
-            copy.wait_recv()
-            got_t[slot] = (
-                mine[i * rows : (i + 1) * rows, :] + got_t[slot].astype(F32)
-            ).astype(BF16)
-            for h in range(cuts if slot else 0):
-                cut = slice(h * part, (h + 1) * part)
-                crossing[slot, h] = go(
-                    got_t.at[slot, :, cut], got_p.at[slot - 1, :, cut], plane_s,
-                    cuts * (slot - 1) + h, there(sp=block),
+        swaps = {}
+        for h in range(cuts):
+            for cut, value in back(blocks, 1 - core, h):
+                for i, block in enumerate(blocks):
+                    slots[whole(block), cut] = value[i * rows : (i + 1) * rows].astype(BF16)
+            cut = slice(h * part, (h + 1) * part)
+            for block, slot in zip(blocks, marks):
+                swaps[slot, h] = go(
+                    slots.at[whole(block), cut], got_t.at[slot, :, cut], twin_s,
+                    cuts * slot + h, twin,
                 )
+        for h in range(cuts):
+            for cut, value in back(blocks, core, h):
+                mine[0 : len(blocks) * rows, cut] = value
+            cut = slice(h * part, (h + 1) * part)
+            for i, (block, slot) in enumerate(zip(blocks, marks)):
+                swaps[slot, h].wait_recv()
+                got_t[slot, :, cut] = (
+                    mine[i * rows : (i + 1) * rows, cut] + got_t[slot, :, cut].astype(F32)
+                ).astype(BF16)
+                if slot:
+                    crossing[slot, h] = go(
+                        got_t.at[slot, :, cut], got_p.at[slot - 1, :, cut], plane_s,
+                        cuts * (slot - 1) + h, there(sp=block),
+                    )
 
     for load in loads[9:]:
         load.wait()
@@ -396,6 +405,27 @@
             go(grad_in.at[kept, to], grad_in.at[kept, to], twin_b, h * depth, twin)
         )
     lax.fori_loop(turns // 2, turns, down, 0)
+    slab = width // n
+    owned = n // 2
+
+    def slab_copy(goal, d, block):
+        return pltpu.make_async_remote_copy(
+            src_ref=grad_in.at[:, ds(goal * slab, slab)],
+            dst_ref=proj_in.at[whole(block)],
+            send_sem=slice_s[0].at[d - 1],
+            recv_sem=slice_s[1].at[d - 1],
+            device_id=there(sp=goal),
+            device_id_type=pl.DeviceIdType.MESH,
+        )
+
+    def each_slab(h, act):
+        for j in range(h * owned // cuts, (h + 1) * owned // cuts):
+            goal = core * owned + j
+
+            @pl.when(goal != me)
+            def _():
+                act(slab_copy(goal, lax.rem(goal - me + n, n), me))
+
     for h in range(cuts):
         to = ds(core * wide + h * part, part)
         for d in range(depth - 1):
@@ -404,9 +434,9 @@
             fifth.append(
                 go(grad_in.at[at, to], grad_in.at[at, to], twin_b, h * depth + d + 1, twin)
             )
+        each_slab(h, lambda copy: copy.start())
     for copy in fifth:
         copy.wait_recv()
-    slab = width // n
     mix = dot(grad_in[...], out_proj[...], NT, None)
     g = mix.astype(BF16)
     scale = DK**-0.5
@@ -418,13 +448,6 @@
             carry = local_g if carry is None else local_g + fall[i, keyed(h), :] * carry
         starts[me, keyed(h), :] = carry.astype(BF16)
     opened = [go(starts.at[me], starts.at[me], begin, d, peers[d]) for d in range(n - 1)]
-    sliced = [
-        go(
-            grad_in.at[ds(core * split, split), ds(lax.rem(me + d + 1, n) * slab, slab)],
-            proj_in.at[half(me)], slice_s, d, peer,
-        )
-        for d, peer in enumerate(peers)
-    ]
     proj_in[whole(me), :] = grad_in[:, ds(me * slab, slab)]
     for h in range(heads):
         gh = g[:, valued(h)]
@@ -443,12 +466,35 @@
         opened[d].wait_recv()
         total = total + factors[d] * starts[lax.rem(me + n - 1 - d, n)].astype(F32)
     after[...] = total
-    relayed = []
-    for d in range(n - 1):
-        sliced[d].wait_recv()
-        at = half(lax.rem(me + n - 1 - d, n))
-        relayed.append(go(proj_in.at[at], proj_in.at[at], slice_t, d, twin))
-    for copy in shared + relayed:
+    holder = lax.div(me, owned)
+
+    def passing(d):
+        at = whole(lax.rem(me + n - d, n))
+        return pltpu.make_async_remote_copy(
+            src_ref=proj_in.at[at],
+            dst_ref=proj_in.at[at],
+            send_sem=slice_t[0].at[d - 1],
+            recv_sem=slice_t[1].at[d - 1],
+            device_id=twin,
+            device_id_type=pl.DeviceIdType.MESH,
+        )
+
+    @pl.when(core == holder)
+    def _():
+        for d in range(1, n):
+            slab_copy(me, d, lax.rem(me + n - d, n)).wait_recv()
+            passing(d).start()
+        for d in range(1, n):
+            passing(d).wait_send()
+
+    @pl.when(core != holder)
+    def _():
+        for d in range(1, n):
+            passing(d).wait_recv()
+
+    for h in range(cuts):
+        each_slab(h, lambda copy: copy.wait_send())
+    for copy in shared:
         copy.wait_recv()
     for copy in started:
         copy.wait_send()
@@ -620,7 +666,7 @@
             (log_decay.shape, F32),
         ],
         sems=[14] + both(
-            links, links, 2 * (groups - 1), groups, CUTS * (groups - 1), CUTS * (depth - 1),
+            links, links, 2 * (groups - 1), CUTS * groups, CUTS * (groups - 1), CUTS * (depth - 1),
             CUTS * (depth - 1), CUTS * depth, groups - 1, groups - 1, groups - 1,
         ),
         ident=1,

time: 66.4 us -> 63.5 us (0.956); the launches traced: 66.2 us -> 62.6 us
  Pallas kernels: 65.5 us -> 61.9 us
    pallas_call x2, Pallas kernels: 65.5 us -> 61.9 us  [call(): pl.pallas_call(kernel, out_shape=[m(s, d) for m, s, d in outs], in_specs=...]
where the time goes in v3:
time: 63.5 us; the launch traced here: 62.6 us
  Pallas kernels  61.9 us (97%)
  between operations  0.69 us (1%)
    pallas_call x2, Pallas kernels, call(): pl.pallas_call(kernel, out_shape=[m(s, d) for m, s, d in outs], in_specs=...  61.9 us

profile of v3, /device:TPU:0, one launch (start us, length us, event | category | flops | bytes accessed | tf_op | source)
XLA Modules:
  0.0 62.6 jit_solution(11808052254372745198)
XLA Ops:
  0.6 0.0 copy-start
  0.6 0.0 copy-start.1
  0.7 0.0 copy-start.2
  0.7 57.3 %shard_map.197 = (bf16[1,2048,768]{2,1,0:T(8,128)(2,1)S(1)}, bf16[1,2048,768]{2,1,0:T(8,128)(2,1)S(1)}, bf16[1,768,2048]{2,1,0:T(8,128)(2,1)S(1)}, bf16[512,256]...) custom-call(bf16[128,2048]{1,0:T(8,128)(2,1)} %moe.1, ...), custom_call_target="tpu_custom_call" | custom-call | flops 10000000000 | bytes 1000000 | tf_op jit(solution)/shard_map/pallas_call | solution.py:560
  58.0 0.0 copy-done
  58.0 0.0 copy-done.1
  58.0 0.0 copy-done.2
  58.0 4.5 %shard_map.198 = (bf16[1,2048,768]{2,1,0:T(8,128)(2,1)}, bf16[1,2048,768]{2,1,0:T(8,128)(2,1)}, bf16[1,768,2048]{2,1,0:T(8,128)(2,1)}, f32[512,256]{1,0:T(8,128)...) custom-call(bf16[1,2048,768]{2,1,0:T(8,128)(2,1)S(1)} %get-tuple-element., ...), custom_call_target="tpu_custom_call" | custom-call | flops 200000000 | bytes 1000000 | tf_op jit(solution)/shard_map/pallas_call | solution.py:560
Async XLA Ops:
  0.6 57.4 %copy-start = (bf16[128,256]{1,0:T(8,128)(2,1)S(1)}, bf16[128,256]{1,0:T(8,128)(2,1)}, u32[]{:S(2)}) copy-start(bf16[128,256]{1,0:T(8,128)(2,1)} %values.1) | copy-start | bytes 196612
  0.6 57.4 %copy-start.1 = (bf16[128,128]{1,0:T(8,128)(2,1)S(1)}, bf16[128,128]{1,0:T(8,128)(2,1)}, u32[]{:S(2)}) copy-start(bf16[128,128]{1,0:T(8,128)(2,1)} %queries.1) | copy-start | bytes 98308
  0.7 57.4 %copy-start.2 = (bf16[128,128]{1,0:T(8,128)(2,1)S(1)}, bf16[128,128]{1,0:T(8,128)(2,1)}, u32[]{:S(2)}) copy-start(bf16[128,128]{1,0:T(8,128)(2,1)} %keys.1) | copy-start | bytes 98308

commit v4 on v3

--- a/solution.py
+++ b/solution.py
@@ -504,7 +504,7 @@
     gate, up, down, all_s, proj_in, after, mid, fall, ends, to_end, ke, dq, dk_p, dv_p,
     queries, keys, values,
     gate_o, up_o, down_o, proj_o, dq_o, dk_o, dv_o, dl_o,
-    proj_v, dq_v, dk_v, dv_v, dl_v, sems,
+    proj_v, dq_v, dk_v, dv_v, dl_v, moved, sems,
 ):
     stores = []
 
@@ -517,16 +517,20 @@
         store(src, dst)
     dq_v[...] = dq[...].astype(BF16)
     store(dq_v, dq_o)
+    proj_v[...] = dot(proj_in[...], all_s[...], TN, None)
+    store(proj_v, proj_o)
     rows, channels = queries.shape
     heads = channels // DK
     wide = values.shape[1] // heads
     ones = jnp.ones((SPAN, wide), F32)
-    upper = triangle(SPAN, True)
+    row = lax.broadcasted_iota(jnp.int32, (rows, rows), 0)
+    col = lax.broadcasted_iota(jnp.int32, (rows, rows), 1)
+    upper = (row <= col) & (lax.div(row, SPAN) == lax.div(col, SPAN))
     g_end = after[...]
     for n in reversed(range(rows // SPAN)):
         at = slice(n * SPAN, (n + 1) * SPAN)
         narrow = g_end.astype(BF16)
-        grown = ends[n] * g_end
+        dl_v[at, :] = dot(ones, ends[n] * g_end, NT)
         for h in range(heads):
             keyed = slice(h * DK, (h + 1) * DK)
             valued = slice(h * wide, (h + 1) * wide)
@@ -534,18 +538,16 @@
                 values[at, valued], narrow[keyed, :], NT, None
             )
             dv = dv_p[at, valued] + dot(ke[at, keyed], narrow[keyed, :], NN, None)
+            moved[at, keyed] = dk
             dk_v[at, keyed] = dk.astype(BF16)
             dv_v[at, valued] = dv.astype(BF16)
-            moved = queries[at, keyed].astype(F32) * dq[at, keyed] - keys[at, keyed].astype(
-                F32
-            ) * dk
-            dl_v[at, keyed] = dot(upper, moved, NN) + dot(ones, grown[keyed, :], NT)
         if n:
             g_end = mid[n] + fall[n] * g_end
-    for src, dst in [(dk_v, dk_o), (dv_v, dv_o), (dl_v, dl_o)]:
-        store(src, dst)
-    proj_v[...] = dot(proj_in[...], all_s[...], TN, None)
-    store(proj_v, proj_o)
+    store(dk_v, dk_o)
+    store(dv_v, dv_o)
+    change = queries[...].astype(F32) * dq[...] - keys[...].astype(F32) * moved[...]
+    dl_v[...] = dl_v[...] + dot(upper.astype(F32), change, NN)
+    store(dl_v, dl_o)
     for copy in stores:
         copy.wait()
 
@@ -689,7 +691,7 @@
         ],
         [fast] * 17,
         (*made, queries, keys, values),
-        scratch=small,
+        scratch=[*small, (log_decay.shape, F32)],
         sems=[8],
     )
 

time: 63.5 us -> 62.9 us (level)
  no operation moved by 1% of the time
where the time goes in v4:
time: 62.9 us; the launch traced here: 62 us
  Pallas kernels  61.3 us (97%)
  between operations  0.69 us (1%)
    pallas_call x2, Pallas kernels, call(): pl.pallas_call(kernel, out_shape=[m(s, d) for m, s, d in outs], in_specs=...  61.3 us

profile of v4, /device:TPU:0, one launch (start us, length us, event | category | flops | bytes accessed | tf_op | source)
XLA Modules:
  0.0 62.0 jit_solution(6982878113325084630)
XLA Ops:
  0.6 0.0 copy-start
  0.6 0.0 copy-start.1
  0.7 0.0 copy-start.2
  0.7 57.3 %shard_map.197 = (bf16[1,2048,768]{2,1,0:T(8,128)(2,1)S(1)}, bf16[1,2048,768]{2,1,0:T(8,128)(2,1)S(1)}, bf16[1,768,2048]{2,1,0:T(8,128)(2,1)S(1)}, bf16[512,256]...) custom-call(bf16[128,2048]{1,0:T(8,128)(2,1)} %moe.1, ...), custom_call_target="tpu_custom_call" | custom-call | flops 10000000000 | bytes 1000000 | tf_op jit(solution)/shard_map/pallas_call | solution.py:562
  58.0 0.0 copy-done
  58.0 0.0 copy-done.1
  58.0 0.0 copy-done.2
  58.0 3.9 %shard_map.198 = (bf16[1,2048,768]{2,1,0:T(8,128)(2,1)}, bf16[1,2048,768]{2,1,0:T(8,128)(2,1)}, bf16[1,768,2048]{2,1,0:T(8,128)(2,1)}, f32[512,256]{1,0:T(8,128)...) custom-call(bf16[1,2048,768]{2,1,0:T(8,128)(2,1)S(1)} %get-tuple-element., ...), custom_call_target="tpu_custom_call" | custom-call | flops 200000000 | bytes 1000000 | tf_op jit(solution)/shard_map/pallas_call | solution.py:562
Async XLA Ops:
  0.6 57.4 %copy-start = (bf16[128,256]{1,0:T(8,128)(2,1)S(1)}, bf16[128,256]{1,0:T(8,128)(2,1)}, u32[]{:S(2)}) copy-start(bf16[128,256]{1,0:T(8,128)(2,1)} %values.1) | copy-start | bytes 196612
  0.6 57.4 %copy-start.1 = (bf16[128,128]{1,0:T(8,128)(2,1)S(1)}, bf16[128,128]{1,0:T(8,128)(2,1)}, u32[]{:S(2)}) copy-start(bf16[128,128]{1,0:T(8,128)(2,1)} %queries.1) | copy-start | bytes 98308
  0.7 57.4 %copy-start.2 = (bf16[128,128]{1,0:T(8,128)(2,1)S(1)}, bf16[128,128]{1,0:T(8,128)(2,1)}, u32[]{:S(2)}) copy-start(bf16[128,128]{1,0:T(8,128)(2,1)} %keys.1) | copy-start | bytes 98308
